TPU v7x, 32 devices: a whole 2x2x4 slice. The times are simulated.
32 devices in a mesh: sp: 8 (over z, x), tp: 4 (over y, core).
Axes of the slice: x: 2, y: 2, z: 4, core: 2. Of those that a mesh axis runs over, the one named last changes fastest.
Arguments:
- inputs: bfloat16 [4096, 4096], P('sp', 'tp'), may hold values from -6 to 6
- w_value: bfloat16 [4096, 4096], P(None, 'tp'), may hold values from -0.09375 to 0.09375
- w_gate: bfloat16 [4096, 4096], P(None, 'tp'), may hold values from -0.09375 to 0.09375
- taps: bfloat16 [31, 4096], P(None, 'tp'), may hold values from -1 to 1
- ln_gain: float32 [4096], P('tp'), may hold values from 0.1 to 1.9
- w_out: bfloat16 [4096, 4096], P(None, 'tp'), may hold values from -0.09375 to 0.09375
- grad_out: bfloat16 [4096, 4096], P('sp', 'tp'), may hold values from -6 to 6
Outputs:
- grad_input: bfloat16 [4096, 4096], P('sp', 'tp')
- grad_value_w: float32 [4096, 4096], P('sp', 'tp')
- grad_gate_w: float32 [4096, 4096], P('sp', 'tp')
- grad_out_w: float32 [4096, 4096], P('sp', 'tp')
- grad_taps: float32 [31, 4096], P(None, 'tp')
- grad_gain: float32 [4096], P('tp')
All inputs are finite; a program needn't handle non-finite values.
Results may differ from a plain program's by a relative error of at most 0.017.
Values may be sent and summed in bfloat16 or wider, within the bound.
A program may use at most 128 MiB of HBM per device.

v0:
```python
import jax
import jax.numpy as jnp
from jax import lax
from jax.sharding import Mesh, PartitionSpec as P


SP = ("outer", "pair")


def shifted(value, steps):
    count = lax.axis_size(SP)
    leading, last = (max(0, -steps), min(count, count - steps))
    return lax.ppermute(value, SP, [(source, source + steps) for source in range(leading, last)])


def with_halo(cells, width):
    head, tail = cells[:width], cells[cells.shape[0] - width :]
    return jnp.concatenate([shifted(tail, 1), cells, shifted(head, -1)], axis=0)


def swap(value):
    return lax.ppermute(value, "pair", [(0, 1), (1, 0)])


def sum_tokens(value):
    count, step = lax.axis_size(SP), 1
    while step < count:
        value = value + lax.ppermute(value, SP, [(i, i ^ step) for i in range(count)])
        step *= 2
    return value


def parity_columns(value, block, parity):
    rows, width = value.shape
    split = value.reshape(rows, width // (2 * block), 2, block)
    return lax.dynamic_index_in_dim(split, parity, 2, keepdims=False).reshape(rows, width // 2)


def contract_tokens(left, right):
    return lax.dot_general(
        left, right, (((0,), (0,)), ((), ())), preferred_element_type=jnp.float32
    )


def contract_channels(left, right):
    return lax.dot_general(
        left, right, (((1,), (1,)), ((), ())), preferred_element_type=jnp.float32
    )


def scatter_rows(value):
    return lax.psum_scatter(
        value.astype(jnp.bfloat16), "outer", scatter_dimension=0, tiled=True
    ).astype(jnp.float32)


def scatter_channels(value):
    count, me = lax.axis_size("tp"), lax.axis_index("tp")
    width = value.shape[1] // count

    def part(owner):
        return lax.dynamic_slice_in_dim(value, lax.rem(owner, count) * width, width, axis=1)

    total = part(me).astype(jnp.float32)
    for step in range(1, count):
        sent = lax.ppermute(part(me + step), "tp", [(i, (i + step) % count) for i in range(count)])
        total = total + sent.astype(jnp.float32)
    return total.astype(jnp.bfloat16)


def local(inputs, w_value, w_gate, taps, ln_gain, w_out, grad_out):
    tok_rows = inputs.shape[0]
    own_width = w_value.shape[1]
    full_width = inputs.shape[1] * lax.axis_size("tp")
    radius = taps.shape[0] // 2
    full_inputs, full_grads = (
        lax.all_gather(inputs, "tp", axis=1, tiled=True),
        lax.all_gather(grad_out, "tp", axis=1, tiled=True),
    )
    own = lax.axis_index("pair")
    block = full_width // lax.axis_size(SP)
    crossing = jnp.concatenate([parity_columns(cells, block, 1 - own) for cells in (grad_out, inputs)], axis=0)
    crossed = lax.all_gather(swap(crossing), "tp", axis=1, tiled=True)
    pair_grads = jnp.concatenate([parity_columns(full_grads, block, own), crossed[:tok_rows]], axis=0)
    own_columns, pair_columns = parity_columns(full_inputs, block, own), crossed[tok_rows:]
    pre_value = jnp.dot(full_inputs, w_value, preferred_element_type=jnp.float32)
    pre_gate = jnp.dot(full_inputs, w_gate, preferred_element_type=jnp.float32)
    gate_sigmoid = jax.nn.sigmoid(pre_gate)
    hidden = (pre_value * gate_sigmoid).astype(jnp.bfloat16)
    padded = with_halo(hidden, radius).astype(jnp.float32)
    tap_values = taps.astype(jnp.float32)
    convolved = jnp.zeros((tok_rows, own_width), jnp.float32)
    for offset in range(taps.shape[0]):
        convolved = convolved + tap_values[offset] * padded[offset : offset + tok_rows]
    sum_first, sum_square = lax.psum(
        (jnp.sum(convolved, axis=1), jnp.sum(convolved * convolved, axis=1)), "tp"
    )
    mean = (sum_first / full_width)[:, None]
    variance = (sum_square / full_width)[:, None] - mean * mean
    inverse = lax.rsqrt(variance + 1e-06)
    normed = (convolved - mean) * inverse
    scaled = normed * ln_gain
    activated = jax.nn.silu(scaled).astype(jnp.bfloat16)
    pair_activated = jnp.concatenate([activated, swap(activated)], axis=0)
    grad_act = jnp.dot(full_grads, w_out, preferred_element_type=jnp.float32)
    sig_scaled = jax.nn.sigmoid(scaled)
    grad_scaled = grad_act * sig_scaled * (1.0 + scaled * (1.0 - sig_scaled))
    gain_part = jnp.sum(grad_scaled * normed, axis=0)
    grad_normed = grad_scaled * ln_gain
    first_sum, second_sum = lax.psum(
        (jnp.sum(grad_normed, axis=1), jnp.sum(grad_normed * normed, axis=1)), "tp"
    )
    grad_conv = inverse * (
        grad_normed
        - (first_sum / full_width)[:, None]
        - normed * (second_sum / full_width)[:, None]
    )
    tap_rows = []
    for offset in range(taps.shape[0]):
        tap_rows.append(jnp.sum(padded[offset : offset + tok_rows] * grad_conv, axis=0))
    token_sums = sum_tokens(jnp.stack(tap_rows + [gain_part], axis=0))
    grad_taps, grad_gain = token_sums[:-1], token_sums[-1]
    spread = jnp.zeros((tok_rows + 2 * radius, own_width), jnp.float32)
    for offset in range(taps.shape[0]):
        spread = spread + tap_values[offset] * jnp.pad(
            grad_conv, ((offset, 2 * radius - offset), (0, 0))
        )
    from_before = shifted(spread[tok_rows + radius :], 1)
    from_after = shifted(spread[:radius], -1)
    grad_hidden = spread[radius : radius + tok_rows]
    grad_hidden = grad_hidden + jnp.pad(from_before, ((0, tok_rows - radius), (0, 0)))
    grad_hidden = grad_hidden + jnp.pad(from_after, ((tok_rows - radius, 0), (0, 0)))
    grad_value = (grad_hidden * gate_sigmoid).astype(jnp.bfloat16)
    grad_gate = (grad_hidden * pre_value * gate_sigmoid * (1.0 - gate_sigmoid)).astype(jnp.bfloat16)
    partial_value = contract_channels(grad_value, w_value) + contract_channels(grad_gate, w_gate)
    grad_input = scatter_channels(partial_value.astype(jnp.bfloat16))
    value_sum = contract_tokens(own_columns, grad_value) + contract_tokens(
        pair_columns, swap(grad_value)
    )
    gate_sum = contract_tokens(own_columns, grad_gate) + contract_tokens(
        pair_columns, swap(grad_gate)
    )
    grad_out_w = scatter_rows(contract_tokens(pair_grads, pair_activated))
    grad_value_w = scatter_rows(value_sum)
    grad_gate_w = scatter_rows(gate_sum)
    return (grad_input, grad_value_w, grad_gate_w, grad_out_w, grad_taps, grad_gain)


def solution(mesh):
    count, across = mesh.devices.shape
    fine = Mesh(mesh.devices.reshape(count // 2, 2, across), ("outer", "pair", "tp"))
    in_specs = (
        P(SP, "tp"),
        P(None, "tp"),
        P(None, "tp"),
        P(None, "tp"),
        P("tp"),
        P(None, "tp"),
        P(SP, "tp"),
    )
    out_specs = (P(SP, "tp"), P(SP, "tp"), P(SP, "tp"), P(SP, "tp"), P(None, "tp"), P("tp"))
    return jax.shard_map(local, mesh=fine, in_specs=in_specs, out_specs=out_specs, check_vma=False)
```

profile of v0, /device:TPU:19, one launch (start us, length us, event | category | flops | bytes accessed | tf_op | source)
XLA Modules:
  0.0 402.1 jit_solution(15717223119894662530)
XLA Ops:
  13.2 23.7 %collective-permute-done.7 = bf16[1024,512]{1,0:T(8,128)(2,1)S(1)} collective-permute-done((bf16[1024,512]{1,0:T(8,128)(2,1)S(1)}, bf16[1024,512]{1,0:T(8,128)(2,1)S(1)}, u32[]{:S(2)}, u32[]{:S(2)}) %collective-permute-start.7) | collective-permute-done | bytes 1048608 | tf_op jit(solution)/shard_map/ppermute | solution.py:22
  37.9 8.2 %all-gather.4.cloned.1.call-done = bf16[512,4096]{0,1:T(8,128)(2,1)} async-done(((bf16[512,1024]{0,1:T(8,128)(2,1)}), bf16[512,4096]{0,1:T(8,128)(2,1)}) %all-gather.4.cloned.1.call-update) | async-done | bytes 4194320 | tf_op jit(solution)/shard_map/all_gather | solution.py:77
  46.1 9.5 %add_divide_fusion.1 = f32[512,1024]{1,0:T(8,128)S(1)} fusion(bf16[512,4096]{0,1:T(8,128)(2,1)} %all-gather.4.cloned.1.call-done, bf16[4096,1024]{1,0:T(8,128)(2,1)} %param.9), kind=kOutput, calls=%fused_computation.58 | convolution fusion | flops 4296540160 | bytes 14680064 | tf_op jit(solution)/shard_map/dot_general | solution.py:87
  55.6 10.4 %multiply_convert_fusion.3 = (bf16[512,1024]{1,0:T(8,128)(2,1)S(1)}, f32[512,1024]{1,0:T(8,128)}) fusion(f32[512,1024]{1,0:T(8,128)S(1)} %add_divide_fusion.1, bf16[512,4096]{0,1:T(8,128)(2,1)S(1)} %copy-done.2, bf16[4096,1024]{1,0:T(8,128)(2,1)} %param.8), kind=kOutput, calls=%fused_computation.57 | convolution fusion | flops 4296015872 | bytes 17825792 | tf_op jit(solution)/shard_map/dot_general | solution.py:86
  75.1 10.6 %multiply_reduce_fusion.33 = (f32[512]{0:T(512)S(1)}, f32[512]{0:T(512)S(1)}, f32[512,1024]{1,0:T(8,128)}) fusion(f32[542,1024]{1,0:T(8,128)S(1)} %maximum_convert_fusion, f32[1024]{0:T(1024)S(1)} %bitcast.159, f32[1024]{0:T(1024)S(1)} %bitcast.157, f32[1024]{0:T(1024)S(1)} %bitcast.155, f32[1024]{0:T(1024)S(1)} %bitcast.153, f32[1024]{0:T(1024)S(1)} %bitcast.151, ...), kind=kLoop, calls=%fused_computation.55 | loop fusion | flops 33553408 | bytes 67239936 | tf_op jit(solution)/shard_map/reduce_sum | solution.py:96
  85.7 18.3 %all-reduce.34 = (f32[512]{0:T(512)S(1)}, f32[512]{0:T(512)S(1)}) all-reduce(f32[512]{0:T(512)S(1)} %get-tuple-element.41, f32[512]{0:T(512)S(1)} %get-tuple-element.40), channel_id=1, replica_groups=mesh['outer'=4,'pair'=2,'tp'=4] {'tp'}, use_global_device_ids=true, to_apply=%region_3.4 | all-reduce | flops 1024 | bytes 8192 | tf_op jit(solution)/shard_map/psum | solution.py:95
  104.1 12.5 %multiply_reduce_fusion = (f32[1024]{0:T(1024)S(1)}, f32[512]{0:T(512)S(1)}, f32[512]{0:T(512)S(1)}, bf16[512,1024]{1,0:T(8,128)(2,1)}, f32[512,1024]{1,0:T(8,128)}) fusion(f32[512,1024]{1,0:T(8,128)} %get-tuple-element.47, f32[512]{0:T(512)S(1)} %get-tuple-element.90, f32[512]{0:T(512)S(1)} %get-tuple-element.89, f32[1024]{0:T(1024)S(1)} %copy-done.18, ...), kind=kOutput, calls=%fused_computation.14 | convolution fusion | flops 4304926720 | bytes 17842176 | tf_op jit(solution)/shard_map/dot_general | solution.py:105
  123.6 16.7 %collective-permute-done.10 = bf16[512,1024]{1,0:T(8,128)(2,1)} collective-permute-done((bf16[512,1024]{1,0:T(8,128)(2,1)}, bf16[512,1024]{1,0:T(8,128)(2,1)}, u32[]{:S(2)}, u32[]{:S(2)}) %collective-permute-start.10) | collective-permute-done | bytes 1048608 | tf_op jit(solution)/shard_map/ppermute | solution.py:22
  140.3 7.8 %fusion.4 = bf16[2048,1024]{1,0:T(8,128)(2,1)} fusion(bf16[512,2048]{1,0:T(8,128)(2,1)S(1)} %slice-done, bf16[512,2048]{1,0:T(8,128)(2,1)S(1)} %copy-done.11, bf16[512,1024]{1,0:T(8,128)(2,1)} %collective-permute-done.10, bf16[512,1024]{1,0:T(8,128)(2,1)} %get-tuple-element.55), kind=kOutput, calls=%fused_computation.7 | convolution fusion | flops 4309647360 | bytes 10485760 | tf_op jit(solution)/shard_map/dot_general | solution.py:40
  148.1 7.1 %all-reduce.33 = (f32[512]{0:T(512)S(1)}, f32[512]{0:T(512)S(1)}) all-reduce(f32[512]{0:T(512)S(1)} %get-tuple-element.38, f32[512]{0:T(512)S(1)} %get-tuple-element.39), channel_id=1, replica_groups=mesh['outer'=4,'pair'=2,'tp'=4] {'tp'}, use_global_device_ids=true, to_apply=%region_7.8 | all-reduce | flops 1024 | bytes 8192 | tf_op jit(solution)/shard_map/psum | solution.py:110
  155.3 6.4 %multiply_reduce_fusion.18 = (f32[1024]{0:T(1024)S(1)}, f32[1024]{0:T(1024)S(1)}, f32[1024]{0:T(1024)S(1)}, f32[1024]{0:T(1024)S(1)}, f32[1024]{0:T(1024)S(1)}, ...) fusion(f32[542,1024]{1,0:T(8,128)S(1)} %maximum_convert_fusion,, ...), kind=kLoop, calls=%fused_computation.32 | loop fusion | flops 17288192 | bytes 33619968 | tf_op jit(solution)/shard_map/reduce_sum | solution.py:120
  161.8 10.2 %multiply_add_fusion = f32[542,1024]{1,0:T(8,128)S(1)} fusion(f32[512,1024]{1,0:T(8,128)S(1)} %get-tuple-element.46, f32[1024]{0:T(1024)S(1)} %bitcast.160, f32[1024]{0:T(1024)S(1)} %bitcast.158, f32[1024]{0:T(1024)S(1)} %bitcast.156, f32[1024]{0:T(1024)S(1)} %bitcast.154, f32[1024]{0:T(1024)S(1)} %bitcast.152, f32[1024]{0:T(1024)S(1)} %bitcast.150, ...), kind=kLoop, calls=%fused_computation.8 | loop fusion | flops 33855488 | bytes 4444160 | tf_op jit(solution)/shard_map/add | solution.py:125
  185.6 21.5 %collective-permute-done.8 = bf16[512,1024]{1,0:T(8,128)(2,1)S(1)} collective-permute-done((bf16[512,1024]{1,0:T(8,128)(2,1)S(1)}, bf16[512,1024]{1,0:T(8,128)(2,1)S(1)}, u32[]{:S(2)}, u32[]{:S(2)}) %collective-permute-start.8) | collective-permute-done | bytes 1048608 | tf_op jit(solution)/shard_map/ppermute | solution.py:22
  209.6 4.4 %add_convert_fusion.1 = bf16[2048,1024]{1,0:T(8,128)(2,1)} fusion(f32[2048,1024]{1,0:T(8,128)S(1)} %fusion.12, bf16[512,2048]{0,1:T(8,128)(2,1)S(1)} %bitcast.93, bf16[512,1024]{1,0:T(8,128)(2,1)S(1)} %get-tuple-element.48), kind=kOutput, calls=%fused_computation.1 | convolution fusion | flops 2151677952 | bytes 15728640 | tf_op jit(solution)/shard_map/dot_general | solution.py:40
  219.9 16.9 %collective-permute-done.9 = bf16[512,1024]{1,0:T(8,128)(2,1)S(1)} collective-permute-done((bf16[512,1024]{1,0:T(8,128)(2,1)}, bf16[512,1024]{1,0:T(8,128)(2,1)S(1)}, u32[]{:S(2)}, u32[]{:S(2)}) %collective-permute-start.9) | collective-permute-done | bytes 1048608 | tf_op jit(solution)/shard_map/ppermute | solution.py:22
  236.9 4.6 %add_convert_fusion = bf16[2048,1024]{1,0:T(8,128)(2,1)} fusion(f32[2048,1024]{1,0:T(8,128)S(1)} %fusion.20, bf16[512,1024]{1,0:T(8,128)(2,1)S(1)} %collective-permute-done.9, bf16[1024,2048]{1,0:T(8,128)(2,1)S(1)} %copy-done.13), kind=kOutput, calls=%fused_computation | convolution fusion | flops 2151677952 | bytes 15728640 | tf_op jit(solution)/shard_map/dot_general | solution.py:40
  241.5 11.5 %fusion.19 = f32[512,4096]{1,0:T(8,128)} fusion(bf16[512,1024]{1,0:T(8,128)(2,1)} %get-tuple-element.49, bf16[4096,1024]{1,0:T(8,128)(2,1)} %param.9), kind=kOutput, calls=%fused_computation.81 | convolution fusion | flops 4294967296 | bytes 17825792 | tf_op jit(solution)/shard_map/dot_general | solution.py:46
  253.0 9.5 %add_convert_fusion.2 = bf16[512,4096]{1,0:T(8,128)(2,1)S(1)} fusion(f32[512,4096]{1,0:T(8,128)} %fusion.19, bf16[512,1024]{1,0:T(8,128)(2,1)S(1)} %get-tuple-element.48, bf16[4096,1024]{1,0:T(8,128)(2,1)} %param.8), kind=kOutput, calls=%fused_computation.2 | convolution fusion | flops 4299161600 | bytes 22020096 | tf_op jit(solution)/shard_map/dot_general | solution.py:46
  270.3 4.6 %multiply_reduce_fusion.1 = (f32[1024]{0:T(1024)S(1)}, f32[1024]{0:T(1024)S(1)}, f32[1024]{0:T(1024)S(1)}, f32[1024]{0:T(1024)S(1)}, f32[1024]{0:T(1024)S(1)}, /...) fusion(f32[512,1024]{1,0:T(8,128)S(1)} %copy-done.1, ...), kind=kLoop, calls=%fused_computation.15 | loop fusion | flops 18855936 | bytes 39919616 | tf_op jit(solution)/shard_map/reduce_sum | solution.py:120
  281.0 8.7 %collective-permute-done.12 = f32[32,1024]{1,0:T(8,128)S(1)} collective-permute-done((f32[32,1024]{1,0:T(8,128)S(1)}, f32[32,1024]{1,0:T(8,128)S(1)}, u32[]{:S(2)}, u32[]{:S(2)}) %collective-permute-start.12) | collective-permute-done | bytes 131104 | tf_op jit(solution)/shard_map/ppermute | solution.py:28
  289.7 8.0 %collective-permute-start.13 = (f32[32,1024]{1,0:T(8,128)S(1)}, f32[32,1024]{1,0:T(8,128)S(1)}, u32[]{:S(2)}, u32[]{:S(2)}) collective-permute-start(f32[32,1024]{1,0:T(8,128)S(1)} %add.426), channel_id=1, source_target_pairs={{0,16},{4,20},{8,24},{12,28},{16,0},{20,4},{24,8},{28,12},{1,17},{... | collective-permute-start | bytes 393224 | tf_op jit(solution)/shard_map/ppermute | solution.py:28
  297.7 11.4 %collective-permute-done.13 = f32[32,1024]{1,0:T(8,128)S(1)} collective-permute-done((f32[32,1024]{1,0:T(8,128)S(1)}, f32[32,1024]{1,0:T(8,128)S(1)}, u32[]{:S(2)}, u32[]{:S(2)}) %collective-permute-start.13) | collective-permute-done | bytes 131104 | tf_op jit(solution)/shard_map/ppermute | solution.py:28
  309.8 5.3 %collective-permute-done.5 = bf16[512,1024]{1,0:T(8,128)(2,1)} collective-permute-done((bf16[512,1024]{1,0:T(8,128)(2,1)S(1)}, bf16[512,1024]{1,0:T(8,128)(2,1)}, u32[]{:S(2)}, u32[]{:S(2)}) %collective-permute-start.5) | collective-permute-done | bytes 1048608 | tf_op jit(solution)/shard_map/ppermute | solution.py:66
  324.8 67.3 %reduce-scatter.6.cloned.1.call-done = bf16[512,1024]{1,0:T(8,128)(2,1)} async-done(((bf16[2048,1024]{1,0:T(8,128)(2,1)}), bf16[512,1024]{1,0:T(8,128)(2,1)}) %reduce-scatter.6.cloned.1.call-update) | async-done | bytes 1048592 | tf_op jit(solution)/shard_map/reduce_scatter | solution.py:52
  (106 shorter events, 72.0 us)
Async XLA Ops:
  7.2 38.9 %all-gather.4.cloned.1.call-start = ((), (), s32[]{:S(2)}) async-start(), calls=%async_computation.3 | async-start | bytes 5242880 | tf_op jit(solution)/shard_map/all_gather | solution.py:77
  9.6 94.4 %all-gather.6.cloned.1.call-start = ((), (), s32[]{:S(2)}) async-start(), calls=%async_computation.4 | async-start | bytes 5242880 | tf_op jit(solution)/shard_map/all_gather | solution.py:78
  11.1 112.5 %all-gather.8.cloned.1.call-start = ((), (), s32[]{:S(2)}) async-start(), calls=%async_computation.5 | async-start | bytes 5242880 | tf_op jit(solution)/shard_map/all_gather | solution.py:83
  12.6 24.2 %collective-permute-start.7 = (bf16[1024,512]{1,0:T(8,128)(2,1)S(1)}, bf16[1024,512]{1,0:T(8,128)(2,1)S(1)}, u32[]{:S(2)}, u32[]{:S(2)}) collective-permute-start(bf16[1024,512]{1,0:T(8,128)(2,1)S(1)} %pad_maximum_fusion), channel_id=1, source_target_pairs={{0,4},{4,0},{1,5},{5,1},{2,6},{6,2},{3,7},{7,3},{8,12},{12,8},{9,1... | collective-permute-start | bytes 3145736 | tf_op jit(solution)/shard_map/ppermute | solution.py:22
  37.8 281.3 %reduce-scatter.8.cloned.1.call-start = ((), (), s32[]{:S(2)}) async-start(), calls=%async_computation.8 | async-start | bytes 5242880 | tf_op jit(solution)/shard_map/reduce_scatter | solution.py:52
  66.1 5.3 %collective-permute-start = (bf16[15,1024]{1,0:T(8,128)(2,1)S(1)}, bf16[15,1024]{1,0:T(8,128)(2,1)S(1)}, u32[]{:S(2)}, u32[]{:S(2)}) collective-permute-start(bf16[15,1024]{1,0:T(8,128)(2,1)S(1)} %get-tuple-element.56), channel_id=1, source_target_pairs={{0,4},{4,8},{8,12},{12,16},{16,20},{20,24},{24,28},{1,5},{5,9},{9,... | collective-permute-start | bytes 92168 | tf_op jit(solution)/shard_map/ppermute | solution.py:13
  69.2 5.6 %collective-permute-start.1 = (bf16[15,1024]{1,0:T(8,128)(2,1)S(1)}, bf16[15,1024]{1,0:T(8,128)(2,1)S(1)}, u32[]{:S(2)}, u32[]{:S(2)}) collective-permute-start(bf16[15,1024]{1,0:T(8,128)(2,1)S(1)} %get-tuple-element.57), channel_id=1, source_target_pairs={{4,0},{8,4},{12,8},{16,12},{20,16},{24,20},{28,24},{5,1},{9,5},{13... | collective-permute-start | bytes 92168 | tf_op jit(solution)/shard_map/ppermute | solution.py:13
  75.1 28.9 %copy-start.18 = (f32[1024]{0:T(1024)S(1)}, f32[1024]{0:T(1024)}, u32[]{:S(2)}) copy-start(f32[1024]{0:T(1024)} %param.11) | copy-start | bytes 12292
  116.5 23.8 %collective-permute-start.10 = (bf16[512,1024]{1,0:T(8,128)(2,1)}, bf16[512,1024]{1,0:T(8,128)(2,1)}, u32[]{:S(2)}, u32[]{:S(2)}) collective-permute-start(bf16[512,1024]{1,0:T(8,128)(2,1)} %get-tuple-element.55), channel_id=1, source_target_pairs={{0,4},{4,0},{1,5},{5,1},{2,6},{6,2},{3,7},{7,3},{8,12},{12,8},{9,1... | collective-permute-start | bytes 3145736 | tf_op jit(solution)/shard_map/ppermute | solution.py:22
  148.1 173.9 %reduce-scatter.4.cloned.1.call-start = ((), (), s32[]{:S(2)}) async-start(), calls=%async_computation.6 | async-start | bytes 5242880 | tf_op jit(solution)/shard_map/reduce_scatter | solution.py:52
  172.0 6.9 %collective-permute-start.2 = (f32[15,1024]{1,0:T(8,128)S(1)}, f32[15,1024]{1,0:T(8,128)S(1)}, u32[]{:S(2)}, u32[]{:S(2)}) collective-permute-start(f32[15,1024]{1,0:T(8,128)S(1)} %get-tuple-element.53), channel_id=1, source_target_pairs={{0,4},{4,8},{8,12},{12,16},{16,20},{20,24},{24,28},{1,5},{5,9},{9,... | collective-permute-start | bytes 184328 | tf_op jit(solution)/shard_map/ppermute | solution.py:13
  174.0 8.0 %collective-permute-start.3 = (f32[15,1024]{1,0:T(8,128)S(1)}, f32[15,1024]{1,0:T(8,128)S(1)}, u32[]{:S(2)}, u32[]{:S(2)}) collective-permute-start(f32[15,1024]{1,0:T(8,128)S(1)} %get-tuple-element.54), channel_id=1, source_target_pairs={{4,0},{8,4},{12,8},{16,12},{20,16},{24,20},{28,24},{5,1},{9,5},{13... | collective-permute-start | bytes 184328 | tf_op jit(solution)/shard_map/ppermute | solution.py:13
  183.8 23.3 %collective-permute-start.8 = (bf16[512,1024]{1,0:T(8,128)(2,1)S(1)}, bf16[512,1024]{1,0:T(8,128)(2,1)S(1)}, u32[]{:S(2)}, u32[]{:S(2)}) collective-permute-start(bf16[512,1024]{1,0:T(8,128)(2,1)S(1)} %get-tuple-element.48), channel_id=1, source_target_pairs={{0,4},{4,0},{1,5},{5,1},{2,6},{6,2},{3,7},{7,3},{8,12},{12,8},{9,1... | collective-permute-start | bytes 3145736 | tf_op jit(solution)/shard_map/ppermute | solution.py:22
  185.5 21.7 %copy-start.12 = (bf16[1024,2048]{1,0:T(8,128)(2,1)S(1)}, bf16[1024,2048]{1,0:T(8,128)(2,1)}, u32[]{:S(2)}) copy-start(bf16[1024,2048]{1,0:T(8,128)(2,1)} %all-gather.8.cloned.1.call-done) | copy-start | bytes 12582916
  185.6 24.0 %copy-start.10 = (bf16[512,4,1,512]{0,3,2,1:T(8,128)(2,1)}, bf16[512,4,1,512]{0,3,2,1:T(8,128)(2,1)S(1)}, u32[]{:S(2)}) copy-start(bf16[512,4,1,512]{0,3,2,1:T(8,128)(2,1)S(1)} %constant_dynamic-slice_fusion.3) | copy-start | bytes 6291460
  214.1 178.0 %reduce-scatter.6.cloned.1.call-start = ((), (), s32[]{:S(2)}) async-start(), calls=%async_computation.7 | async-start | bytes 5242880 | tf_op jit(solution)/shard_map/reduce_scatter | solution.py:52
  214.3 22.6 %copy-start.13 = (bf16[1024,2048]{1,0:T(8,128)(2,1)S(1)}, bf16[1024,2048]{1,0:T(8,128)(2,1)}, u32[]{:S(2)}) copy-start(bf16[1024,2048]{1,0:T(8,128)(2,1)} %all-gather.8.cloned.1.call-done) | copy-start | bytes 12582916
  214.3 22.6 %collective-permute-start.9 = (bf16[512,1024]{1,0:T(8,128)(2,1)}, bf16[512,1024]{1,0:T(8,128)(2,1)S(1)}, u32[]{:S(2)}, u32[]{:S(2)}) collective-permute-start(bf16[512,1024]{1,0:T(8,128)(2,1)} %get-tuple-element.49), channel_id=1, source_target_pairs={{0,4},{4,0},{1,5},{5,1},{2,6},{6,2},{3,7},{7,3},{8,12},{12,8},{9,1... | collective-permute-start | bytes 3145736 | tf_op jit(solution)/shard_map/ppermute | solution.py:22
  265.4 44.4 %collective-permute-start.4 = (bf16[512,1024]{1,0:T(8,128)(2,1)}, bf16[512,1024]{1,0:T(8,128)(2,1)}, u32[]{:S(2)}, u32[]{:S(2)}) collective-permute-start(bf16[512,1024]{1,0:T(8,128)(2,1)} %get-tuple-element.50), channel_id=1, source_target_pairs={{0,1},{1,2},{2,3},{3,0},{4,5},{5,6},{6,7},{7,4},{8,9},{9,10},{10,1... | collective-permute-start | bytes 3145736 | tf_op jit(solution)/shard_map/ppermute | solution.py:66
  269.2 40.6 %collective-permute-start.6 = (bf16[512,1024]{1,0:T(8,128)(2,1)}, bf16[512,1024]{1,0:T(8,128)(2,1)}, u32[]{:S(2)}, u32[]{:S(2)}) collective-permute-start(bf16[512,1024]{1,0:T(8,128)(2,1)} %get-tuple-element.51), channel_id=1, source_target_pairs={{0,3},{1,0},{2,1},{3,2},{4,7},{5,4},{6,5},{7,6},{8,11},{9,8},{10,9... | collective-permute-start | bytes 3145736 | tf_op jit(solution)/shard_map/ppermute | solution.py:66
  269.4 45.7 %collective-permute-start.5 = (bf16[512,1024]{1,0:T(8,128)(2,1)S(1)}, bf16[512,1024]{1,0:T(8,128)(2,1)}, u32[]{:S(2)}, u32[]{:S(2)}) collective-permute-start(bf16[512,1024]{1,0:T(8,128)(2,1)S(1)} %get-tuple-element.52), channel_id=1, source_target_pairs={{0,2},{1,3},{2,0},{3,1},{4,6},{5,7},{6,4},{7,5},{8,10},{9,11},{10,... | collective-permute-start | bytes 3145736 | tf_op jit(solution)/shard_map/ppermute | solution.py:66
  275.2 4.3 %collective-permute-start.11 = (f32[32,1024]{1,0:T(8,128)S(1)}, f32[32,1024]{1,0:T(8,128)S(1)}, u32[]{:S(2)}, u32[]{:S(2)}) collective-permute-start(f32[32,1024]{1,0:T(8,128)S(1)} %stack.131), channel_id=1, source_target_pairs={{0,4},{4,0},{8,12},{12,8},{16,20},{20,16},{24,28},{28,24},{1,5},{5... | collective-permute-start | bytes 393224 | tf_op jit(solution)/shard_map/ppermute | solution.py:28
  279.5 10.2 %collective-permute-start.12 = (f32[32,1024]{1,0:T(8,128)S(1)}, f32[32,1024]{1,0:T(8,128)S(1)}, u32[]{:S(2)}, u32[]{:S(2)}) collective-permute-start(f32[32,1024]{1,0:T(8,128)S(1)} %add.425), channel_id=1, source_target_pairs={{0,8},{4,12},{8,0},{12,4},{16,24},{20,28},{24,16},{28,20},{1,9},{5... | collective-permute-start | bytes 393224 | tf_op jit(solution)/shard_map/ppermute | solution.py:28
  289.7 19.4 %collective-permute-start.13 = (f32[32,1024]{1,0:T(8,128)S(1)}, f32[32,1024]{1,0:T(8,128)S(1)}, u32[]{:S(2)}, u32[]{:S(2)}) collective-permute-start(f32[32,1024]{1,0:T(8,128)S(1)} %add.426), channel_id=1, source_target_pairs={{0,16},{4,20},{8,24},{12,28},{16,0},{20,4},{24,8},{28,12},{1,17},{... | collective-permute-start | bytes 393224 | tf_op jit(solution)/shard_map/ppermute | solution.py:28
  (16 other events, 135.2 us)
Sparse Core Ops, SparseCore 0:
  10.1 35.8 all-gather.3
  47.6 34.4 all-gather.5
  83.7 34.6 all-gather.7
  148.2 78.0 reduce-scatter.7
  228.5 84.0 reduce-scatter.3
  314.8 77.2 reduce-scatter.5
where the time goes:
time: 405 us; the launch traced here: 402 us
  waiting for transfers between devices  191 us (47%)
  matrix products  77 us (19%)
  other arithmetic  46.7 us (12%)
  starting transfers between devices  29.9 us (7%)
  blocking collectives  25.5 us (6%)
  local copies, waits for them, and re-layouts  17.4 us (4%)
  between operations  14.9 us (4%)
    ppermute x4, waiting for transfers between devices, swap(): return lax.ppermute(value, 'pair', [(0, 1), (1, 0)])  78.8 us
    reduce_scatter x3, waiting for transfers between devices, scatter_rows(): lax.psum_scatter(value.astype(jnp.bfloat16), 'outer', scatter_dimension=0...  67.3 us
    dot_general x5, matrix products, contract_tokens(): lax.dot_general(left, right, (((0,), (0,)), ((), ())), preferred_element_...  23.5 us
    ppermute x3, waiting for transfers between devices, sum_tokens(): lax.ppermute(value, SP, [(i, i ^ step) for i in range(count)])  23.2 us
    dot_general x2, matrix products, contract_channels(): lax.dot_general(left, right, (((1,), (1,)), ((), ())), preferred_element_...  21 us
    psum x1, blocking collectives, local(): lax.psum((jnp.sum(convolved, axis=1), jnp.sum(convolved * convolved, axis...  18.3 us
    dot_general x1, matrix products, local(): grad_act = jnp.dot(full_grads, w_out, preferred_element_type=jnp.float32)  12.5 us
    reduce_sum x2, other arithmetic, local(): jnp.sum(padded[offset:offset + tok_rows] * grad_conv, axis=0)  11.1 us
  transfers between devices with their start and end apart: 20, of which 13 were waited for; matrix products, arithmetic and copies ran while one was open for 31% of the time, Pallas kernels for 0%

commit v1 on v0

v1 whole, which is shorter than its diff:
```python
import functools

import jax
import jax.numpy as jnp
from jax import lax
from jax.experimental import pallas as pl
from jax.experimental.pallas import tpu as pltpu
from jax.sharding import Mesh, PartitionSpec as P

MESH = pl.DeviceIdType.MESH
SP = ("outer", "pair")
AXES = ("outer", "pair", "tp")
LANES = 128
PAD = 16
ROWS = 64
F32, BF16 = jnp.float32, jnp.bfloat16


def sigmoid(value):
    return 1.0 / (1.0 + jnp.exp(-value))


def dot(left, right):
    return jnp.dot(left, right, preferred_element_type=F32)


class Sends:
    def __init__(self, sems):
        self.sems, self.open = sems, []

    def start(self, src, dst, recv, device):
        copy = pltpu.make_async_remote_copy(
            src_ref=src, dst_ref=dst, send_sem=self.sems.at[len(self.open)],
            recv_sem=recv, device_id=device, device_id_type=MESH,
        )
        copy.start()
        self.open.append((copy, None))

    def start_if(self, cond, src, dst, recv, device):
        copy = pltpu.make_async_remote_copy(
            src_ref=src, dst_ref=dst, send_sem=self.sems.at[len(self.open)],
            recv_sem=recv, device_id=device, device_id_type=MESH,
        )
        pl.when(cond)(copy.start)
        self.open.append((copy, cond))

    def drain(self):
        for copy, cond in self.open:
            if cond is None:
                copy.wait_send()
            else:
                pl.when(cond)(copy.wait_send)


def arrived(ref, recv):
    pltpu.make_async_copy(ref, ref, recv).wait()


def front_kernel(
    n_outer, n_tp, conv,
    x_ref, g_ref, wv_ref, wg_ref, wo_ref, taps_ref, gain_ref,
    xg_out, gg_out, px_out, pg_out, act_out, gv_out, gt_out, small_out,
    xg, gg, wv, wg, wo, pv, ps, ga, cv, hp, gc, act, gv, gt, small,
    sum_a, sum_b, mean_b, inv_b, stat1, stat2,
    send_sems, recv_x, recv_g, recv_px, recv_pg, recv_h, recv_c, recv_s1, recv_s2, load_sems, own_sems, out_sems,
):
    outer, pair, tp = (lax.axis_index(name) for name in AXES)
    seq, n_seq, per = outer * 2 + pair, n_outer * 2, (n_outer * 2) // n_tp
    tokens, width = xg.shape[1], xg.shape[2]
    n_lane, total = pv.shape[0], width * n_seq
    sibling = tp + 1 - 2 * lax.rem(tp, 2)
    core, n_y = lax.rem(tp, 2), n_tp // 2
    across = [lax.rem(tp + 2 * step, n_tp) for step in range(1, n_y)]
    radius = conv // 2
    before, after = seq - 1, seq + 1
    has_before, has_after = seq > 0, seq < n_seq - 1
    home = lambda index: (outer, pair, index)
    beside = lambda index: (lax.div(index, 2), lax.rem(index, 2), tp)
    facing = (outer, 1 - pair, tp)

    barrier = pltpu.get_barrier_semaphore()

    def greet(device):
        pl.semaphore_signal(barrier, inc=1, device_id=device, device_id_type=MESH)

    for step in range(1, n_tp):
        greet(home(lax.rem(tp + step, n_tp)))
    pl.when(has_before)(lambda: greet(beside(before)))
    pl.when(has_after)(lambda: greet(beside(after)))
    greet(facing)

    block = lambda b, h: b * per + h
    order = [tp, sibling]
    for other in across:
        order += [other, other + 1 - 2 * core]
    loads = []
    for name, (hbm, vmem) in enumerate(((wv_ref, wv), (wg_ref, wg), (wo_ref, wo))):
        loads.append([])
        for rank, b in enumerate(order):
            for h in range(per):
                index = block(b, h)
                row = pl.multiple_of(index * width, width)
                loads[-1].append(
                    pltpu.make_async_copy(hbm.at[pl.ds(row, width), :], vmem.at[index], load_sems.at[name, rank * per + h])
                )
    owns = []
    for name, (hbm, vmem) in enumerate(((x_ref, xg), (g_ref, gg))):
        owns.append([])
        for h in range(per):
            owns[-1].append(
                pltpu.make_async_copy(hbm.at[:, pl.ds(h * width, width)], vmem.at[block(tp, h)], own_sems.at[name, h])
            )
    for copy in owns[0]:
        copy.start()
    for step in range(2 * per):
        loads[0][step].start()
        loads[1][step].start()
    for copy in owns[1]:
        copy.start()
    for step in range(2 * per):
        loads[2][step].start()
    for step in range(2 * per, n_tp * per):
        loads[0][step].start()
        loads[1][step].start()
    for step in range(2 * per, n_tp * per):
        loads[2][step].start()

    count = n_tp - 1 + 1 + has_before.astype(jnp.int32) + has_after.astype(jnp.int32)
    pl.semaphore_wait(barrier, count)

    sends = Sends(send_sems)
    for hbm, vmem, recv in ((x_ref, xg, recv_x), (g_ref, gg, recv_g)):
        for h in range(per):
            src, index = hbm.at[:, pl.ds(h * width, width)], block(tp, h)
            for other in [sibling] + across:
                sends.start(src, vmem.at[index], recv.at[index], home(other))
    crossing = pl.multiple_of((1 - pair) * width, width)
    sends.start(x_ref.at[:, pl.ds(crossing, width)], px_out.at[tp], recv_px.at[tp], facing)
    sends.start(g_ref.at[:, pl.ds(crossing, width)], pg_out.at[tp], recv_pg.at[tp], facing)

    def project(ranks, left, pairs, first):
        def body(j, carry):
            column = pl.multiple_of(j * 256, 256)
            for weight, result in pairs:
                value = None
                for rank in ranks:
                    b, h = order[rank // per], rank % per
                    index = block(b, h)
                    part = dot(left[index], weight[index, :, pl.ds(column, 256)])
                    value = part if value is None else value + part
                for half in range(2):
                    piece = value[:, half * LANES : (half + 1) * LANES]
                    if first:
                        result[2 * j + half] = piece
                    else:
                        result[2 * j + half] += piece
            return carry

        lax.fori_loop(0, n_lane // 2, body, 0)

    def ready(ranks, names):
        for rank in ranks:
            for name in names:
                loads[name][rank].wait()

    near = list(range(per))
    side = list(range(per, 2 * per))
    for copy in owns[0]:
        copy.wait()
    ready(near, (0, 1))
    project(near, xg, ((wv, pv), (wg, ps)), True)
    for rank in side:
        index = block(sibling, rank % per)
        arrived(xg.at[index], recv_x.at[index])
    ready(side, (0, 1))
    project(side, xg, ((wv, pv), (wg, ps)), False)
    for copy in owns[1]:
        copy.wait()
    for rank in side:
        index = block(sibling, rank % per)
        arrived(gg.at[index], recv_g.at[index])
    ready(near + side, (2,))
    project(near + side, gg, ((wo, ga),), True)

    def land(vmem, recv, b, h, crossed, recv_crossed):
        index = block(b, h)
        arrived(vmem.at[index], recv.at[index])
        sends.start(vmem.at[index], vmem.at[index], recv.at[index], home(sibling))
        sends.start_if(h != pair, vmem.at[index], crossed.at[b], recv_crossed.at[b], facing)

    for step, other in enumerate(across):
        for h in range(per):
            land(xg, recv_x, other, h, px_out, recv_px)
            rank = (2 + 2 * step) * per + h
            ready([rank], (0, 1))
            project([rank], xg, ((wv, pv), (wg, ps)), False)
            twin, index = rank + per, block(other + 1 - 2 * core, h)
            arrived(xg.at[index], recv_x.at[index])
            ready([twin], (0, 1))
            project([twin], xg, ((wv, pv), (wg, ps)), False)

    def gate(i, carry):
        c, r = lax.div(i, tokens // ROWS), lax.rem(i, tokens // ROWS)
        rows = pl.ds(pl.multiple_of(r * ROWS, ROWS), ROWS)
        sig = sigmoid(ps[c, rows, :])
        ps[c, rows, :] = sig
        hp[c, pl.ds(pl.multiple_of(r * ROWS + PAD, 8), ROWS), :] = (pv[c, rows, :] * sig).astype(BF16).astype(F32)
        return carry

    lax.fori_loop(0, n_lane * (tokens // ROWS), gate, 0)

    def halo(buffer, recv):
        @pl.when(jnp.logical_not(has_before))
        def _():
            buffer[:, 0:PAD, :] = jnp.zeros((n_lane, PAD, LANES), F32)

        @pl.when(jnp.logical_not(has_after))
        def _():
            buffer[:, PAD + tokens : 2 * PAD + tokens, :] = jnp.zeros((n_lane, PAD, LANES), F32)

        sends.start_if(has_after, buffer.at[:, pl.ds(tokens, PAD), :], buffer.at[:, pl.ds(0, PAD), :], recv.at[0], beside(after))
        sends.start_if(has_before, buffer.at[:, pl.ds(PAD, PAD), :], buffer.at[:, pl.ds(PAD + tokens, PAD), :], recv.at[1], beside(before))

    def halo_here(buffer, recv):
        pl.when(has_before)(lambda: arrived(buffer.at[:, pl.ds(0, PAD), :], recv.at[0]))
        pl.when(has_after)(lambda: arrived(buffer.at[:, pl.ds(PAD + tokens, PAD), :], recv.at[1]))

    halo(hp, recv_h)

    def convolve(r):
        rows = pl.ds(pl.multiple_of(r * ROWS, ROWS), ROWS)

        def lane(c, carry):
            first, second = carry
            value = jnp.zeros((ROWS, LANES), F32)
            for k in range(conv):
                value = value + taps_ref[c, k : k + 1, :] * hp[c, pl.ds(r * ROWS + (PAD + k - radius), ROWS), :]
            cv[c, rows, :] = value
            return first + value, second + value * value

        zero = jnp.zeros((ROWS, LANES), F32)
        first, second = lax.fori_loop(0, n_lane, lane, (zero, zero))
        sum_a[rows, :] = first
        sum_b[rows, :] = second

    def inner_rows(body):
        def step(r, carry):
            body(r)
            return carry

        lax.fori_loop(1, tokens // ROWS - 1, step, 0)

    inner_rows(convolve)
    halo_here(hp, recv_h)
    convolve(0)
    convolve(tokens // ROWS - 1)

    def to_row(value):
        return jnp.sum(value.T, axis=0, keepdims=True)

    def to_rows(row):
        return jnp.broadcast_to(row, (LANES, tokens)).T

    def send_sums(stat, recv):
        stat[tp, 0:1, :] = to_row(sum_a[...])
        stat[tp, 1:2, :] = to_row(sum_b[...])
        for step in range(1, n_tp):
            sends.start(stat.at[tp], stat.at[tp], recv.at[tp], home(lax.rem(tp + step, n_tp)))

    def take_sums(stat, recv):
        for step in range(1, n_tp):
            other = lax.rem(tp + step, n_tp)
            arrived(stat.at[other], recv.at[other])
        first, second = stat[0, 0:1, :], stat[0, 1:2, :]
        for other in range(1, n_tp):
            first, second = first + stat[other, 0:1, :], second + stat[other, 1:2, :]
        return first / total, second / total

    send_sums(stat1, recv_s1)

    for step, other in enumerate(across):
        for h in range(per):
            land(gg, recv_g, other, h, pg_out, recv_pg)
            rank = (2 + 2 * step) * per + h
            twin, index = rank + per, block(other + 1 - 2 * core, h)
            arrived(gg.at[index], recv_g.at[index])
            ready([rank, twin], (2,))
            project([rank, twin], gg, ((wo, ga),), False)

    mean, square = take_sums(stat1, recv_s1)
    mean_b[...] = to_rows(mean)
    inv_b[...] = to_rows(lax.rsqrt(square - mean * mean + 1e-06))
    small[:, conv : conv + 1, :] = jnp.zeros((n_lane, 1, LANES), F32)

    def backward(r, carry):
        rows = pl.ds(pl.multiple_of(r * ROWS, ROWS), ROWS)
        mean_r, inv_r = mean_b[rows, :], inv_b[rows, :]

        def lane(c, carry):
            first, second = carry
            normed = (cv[c, rows, :] - mean_r) * inv_r
            cv[c, rows, :] = normed
            gain = gain_ref[c]
            scaled = normed * gain
            sig = sigmoid(scaled)
            act[rows, pl.ds(pl.multiple_of(c * LANES, LANES), LANES)] = (scaled * sig).astype(BF16)
            grad_scaled = ga[c, rows, :] * sig * (1.0 + scaled * (1.0 - sig))
            small[c, conv : conv + 1, :] += jnp.sum(grad_scaled * normed, axis=0, keepdims=True)
            grad_normed = grad_scaled * gain
            gc[c, pl.ds(pl.multiple_of(r * ROWS + PAD, 8), ROWS), :] = grad_normed
            return first + grad_normed, second + grad_normed * normed

        zero = jnp.zeros((ROWS, LANES), F32)
        first, second = lax.fori_loop(0, n_lane, lane, (zero, zero))
        sum_a[rows, :] = first
        sum_b[rows, :] = second
        return carry

    lax.fori_loop(0, tokens // ROWS, backward, 0)
    send_sums(stat2, recv_s2)
    outs = [pltpu.make_async_copy(act, act_out, out_sems.at[0])]
    outs[0].start()
    first_mean, second_mean = take_sums(stat2, recv_s2)
    sum_a[...] = to_rows(first_mean)
    sum_b[...] = to_rows(second_mean)

    def finish(r):
        rows = pl.ds(pl.multiple_of(r * ROWS, ROWS), ROWS)
        padded = pl.ds(pl.multiple_of(r * ROWS + PAD, 8), ROWS)
        inv_r, first_r, second_r = inv_b[rows, :], sum_a[rows, :], sum_b[rows, :]

        def lane(c, carry):
            gc[c, padded, :] = inv_r * (gc[c, padded, :] - first_r - cv[c, rows, :] * second_r)
            return carry

        lax.fori_loop(0, n_lane, lane, 0)

    finish(0)
    finish(tokens // ROWS - 1)
    halo(gc, recv_c)
    inner_rows(finish)

    def spread(r):
        rows = pl.ds(pl.multiple_of(r * ROWS, ROWS), ROWS)

        def lane(c, carry):
            value = jnp.zeros((ROWS, LANES), F32)
            for k in range(conv):
                value = value + taps_ref[c, k : k + 1, :] * gc[c, pl.ds(r * ROWS + (PAD + radius - k), ROWS), :]
            sig = ps[c, rows, :]
            columns = pl.ds(pl.multiple_of(c * LANES, LANES), LANES)
            lead = value * sig
            gv[rows, columns] = lead.astype(BF16)
            gt[rows, columns] = (value * pv[c, rows, :] * sig * (1.0 - sig)).astype(BF16)
            return carry

        lax.fori_loop(0, n_lane, lane, 0)

    inner_rows(spread)
    halo_here(gc, recv_c)
    spread(0)
    spread(tokens // ROWS - 1)
    outs.append(pltpu.make_async_copy(gv, gv_out, out_sems.at[1]))
    outs.append(pltpu.make_async_copy(gt, gt_out, out_sems.at[2]))
    outs.append(pltpu.make_async_copy(xg, xg_out, out_sems.at[3]))
    outs.append(pltpu.make_async_copy(gg, gg_out, out_sems.at[4]))
    for copy in outs[1:]:
        copy.start()

    mine = [tp] + across
    for crossed, recv in ((px_out, recv_px), (pg_out, recv_pg)):
        for b in mine:
            arrived(crossed.at[b], recv.at[b])
            sends.start(crossed.at[b], crossed.at[b], recv.at[b], home(sibling))

    def tap_sums(c, carry):
        def step(r, sums):
            row = pl.multiple_of(r * 8, 8)
            grad = gc[c, pl.ds(pl.multiple_of(row + PAD, 8), 8), :]
            return tuple(sums[k] + hp[c, pl.ds(row + (PAD + k - radius), 8), :] * grad for k in range(conv))

        sums = lax.fori_loop(0, tokens // 8, step, tuple(jnp.zeros((8, LANES), F32) for _ in range(conv)))
        for k in range(conv):
            small[c, k : k + 1, :] = jnp.sum(sums[k], axis=0, keepdims=True)
        return carry

    lax.fori_loop(0, n_lane, tap_sums, 0)
    outs.append(pltpu.make_async_copy(small, small_out, out_sems.at[5]))
    outs[-1].start()
    for crossed, recv in ((px_out, recv_px), (pg_out, recv_pg)):
        for b in mine:
            twin = b + 1 - 2 * core
            arrived(crossed.at[twin], recv.at[twin])
    sends.drain()
    for copy in outs:
        copy.wait()


def front(inputs, w_value, w_gate, taps, ln_gain, w_out, grad_out):
    n_outer, n_tp = lax.axis_size("outer"), lax.axis_size("tp")
    n_seq = n_outer * 2
    tokens, own = inputs.shape
    conv, channels = taps.shape
    width = own * n_tp // n_seq
    per, n_lane, n_y = n_seq // n_tp, channels // LANES, n_tp // 2
    tap_cells = jnp.pad(taps.astype(F32), ((0, 1), (0, 0))).reshape(conv + 1, n_lane, LANES).transpose(1, 0, 2)
    gain_cells = ln_gain.reshape(n_lane, 1, LANES)
    n_sends = 2 * (per * n_y + 1 + (n_y - 1) * per * 2 + n_y) + 4 + 2 * (n_tp - 1)
    any_spec, vmem_spec = pl.BlockSpec(memory_space=pl.ANY), pl.BlockSpec(memory_space=pltpu.VMEM)
    lanes = lambda rows, dtype=F32: pltpu.VMEM((n_lane, rows, LANES), dtype)
    dma = lambda *shape: pltpu.SemaphoreType.DMA(shape)
    out_shapes = [
        ((n_seq, tokens, width), BF16), ((n_seq, tokens, width), BF16),
        ((n_tp, tokens, width), BF16), ((n_tp, tokens, width), BF16),
        ((tokens, channels), BF16), ((tokens, channels), BF16), ((tokens, channels), BF16),
        ((n_lane, conv + 1, LANES), F32),
    ]
    flops = 2 * 3 * tokens * own * n_tp * channels
    return pl.pallas_call(
        functools.partial(front_kernel, n_outer, n_tp, conv),
        name="front",
        out_shape=[jax.ShapeDtypeStruct(shape, dtype) for shape, dtype in out_shapes],
        in_specs=[any_spec] * 5 + [vmem_spec] * 2,
        out_specs=[any_spec] * len(out_shapes),
        scratch_shapes=[
            pltpu.VMEM((n_seq, tokens, width), BF16), pltpu.VMEM((n_seq, tokens, width), BF16),
            *[pltpu.VMEM((n_seq, width, channels), BF16)] * 3,
            lanes(tokens), lanes(tokens), lanes(tokens), lanes(tokens),
            lanes(tokens + 2 * PAD), lanes(tokens + 2 * PAD),
            *[pltpu.VMEM((tokens, channels), BF16)] * 3,
            lanes(conv + 1),
            *[pltpu.VMEM((tokens, LANES), F32)] * 4,
            *[pltpu.VMEM((n_tp, 8, tokens), F32)] * 2,
            dma(n_sends), dma(n_seq), dma(n_seq), dma(n_tp), dma(n_tp), dma(2), dma(2), dma(n_tp), dma(n_tp),
            dma(3, n_seq), dma(2, per), dma(6),
        ],
        compiler_params=pltpu.CompilerParams(
            collective_id=0, has_side_effects=True, vmem_limit_bytes=63 * 1024 * 1024
        ),
        cost_estimate=pl.CostEstimate(flops=flops, bytes_accessed=40 * 2**20, transcendentals=0),
    )(inputs, grad_out, w_value, w_gate, w_out, tap_cells, gain_cells)


def sum_tokens(value):
    count, step = lax.axis_size(SP), 1
    while step < count:
        value = value + lax.ppermute(value, SP, [(i, i ^ step) for i in range(count)])
        step *= 2
    return value


def swap(value):
    return lax.ppermute(value, "pair", [(0, 1), (1, 0)])


def contract_channels(left, right):
    return lax.dot_general(left, right, (((1,), (1,)), ((), ())), preferred_element_type=F32)


def contract_tokens(left, right):
    value = lax.dot_general(left, right, (((1,), (0,)), ((), ())), preferred_element_type=F32)
    return value.reshape(-1, value.shape[-1])


def scatter_rows(value):
    return lax.psum_scatter(value.astype(BF16), "outer", scatter_dimension=0, tiled=True).astype(F32)


def scatter_channels(value):
    count, me = lax.axis_size("tp"), lax.axis_index("tp")
    width = value.shape[1] // count

    def part(owner):
        return lax.dynamic_slice_in_dim(value, lax.rem(owner, count) * width, width, axis=1)

    total = part(me).astype(F32)
    for step in range(1, count):
        sent = lax.ppermute(part(me + step), "tp", [(i, (i + step) % count) for i in range(count)])
        total = total + sent.astype(F32)
    return total.astype(BF16)


def local(inputs, w_value, w_gate, taps, ln_gain, w_out, grad_out):
    xg, gg, px, pg, activated, grad_value, grad_gate, small = front(
        inputs, w_value, w_gate, taps, ln_gain, w_out, grad_out
    )
    own = lax.axis_index("pair")
    conv = taps.shape[0]

    def mine(cells):
        split = cells.reshape(cells.shape[0] // 2, 2, *cells.shape[1:])
        return lax.dynamic_index_in_dim(split, own, 1, keepdims=False)

    pair_activated = swap(activated)
    pair_value, pair_gate = swap(grad_value), swap(grad_gate)
    token_sums = sum_tokens(small.transpose(1, 0, 2).reshape(conv + 1, -1))
    grad_taps, grad_gain = token_sums[:-1], token_sums[-1]
    grad_out_w = scatter_rows(contract_tokens(mine(gg), activated) + contract_tokens(pg, pair_activated))
    grad_value_w = scatter_rows(contract_tokens(mine(xg), grad_value) + contract_tokens(px, pair_value))
    grad_gate_w = scatter_rows(contract_tokens(mine(xg), grad_gate) + contract_tokens(px, pair_gate))
    partial_value = contract_channels(grad_value, w_value) + contract_channels(grad_gate, w_gate)
    grad_input = scatter_channels(partial_value.astype(BF16))
    return (grad_input, grad_value_w, grad_gate_w, grad_out_w, grad_taps, grad_gain)


def solution(mesh):
    count, across = mesh.devices.shape
    fine = Mesh(mesh.devices.reshape(count // 2, 2, across), AXES)
    in_specs = (P(SP, "tp"), P(None, "tp"), P(None, "tp"), P(None, "tp"), P("tp"), P(None, "tp"), P(SP, "tp"))
    out_specs = (P(SP, "tp"), P(SP, "tp"), P(SP, "tp"), P(SP, "tp"), P(None, "tp"), P("tp"))
    return jax.shard_map(local, mesh=fine, in_specs=in_specs, out_specs=out_specs, check_vma=False)
```

time: 405 us -> 375 us (0.926)
  Pallas kernels: 0 us -> 79 us
  other arithmetic: 46.7 us -> 13.6 us
  matrix products: 77 us -> 45.5 us
  blocking collectives: 25.5 us -> 0 us
  starting transfers between devices: 29.9 us -> 7.02 us
  waiting for transfers between devices: 191 us -> 198 us
    pallas_call x0 -> x1, Pallas kernels: none -> 79 us  [front(): pl.pallas_call(functools.partial(front_kernel, n_outer, n_tp, conv), name...]
    dot_general x8 -> x6, matrix products: 55.9 us -> 25.9 us  [contract_tokens(): lax.dot_general(left, right, (((1,), (0,)), ((), ())), preferred_element_...]
    reduce_scatter x3, waiting for transfers between devices: 67.3 us -> 93.8 us  [scatter_rows(): lax.psum_scatter(value.astype(BF16), 'outer', scatter_dimension=0, tiled=...]
    psum x2 -> x0, blocking collectives: 25.5 us -> none  [the longest x1 18.3 us: local(): lax.psum((jnp.sum(convolved, axis=1), jnp.sum(convolved * convolved, axis...]
    reduce_sum x3 -> x0, other arithmetic: 21.7 us -> none  [the longest x2 11.1 us: local(): jnp.sum(padded[offset:offset + tok_rows] * grad_conv, axis=0)]
    ppermute x4 -> x3, waiting for transfers between devices: 78.8 us -> 61.3 us  [swap(): return lax.ppermute(value, 'pair', [(0, 1), (1, 0)])]
    ppermute x3, waiting for transfers between devices: 5.3 us -> 17.7 us  [scatter_channels(): lax.ppermute(part(me + step), 'tp', [(i, (i + step) % count) for i in ran...]
    ppermute x4 -> x0, starting transfers between devices: 10.6 us -> none  [shifted(): lax.ppermute(value, SP, [(source, source + steps) for source in range(lea...]
  transfers between devices with their start and end apart: 20 -> 12, of which waited for: 13 -> 9; matrix products, arithmetic and copies ran while one was open for 31% -> 16% of each run, Pallas kernels for 0% -> 0%
where the time goes in v1:
time: 375 us; the launch traced here: 373 us
  waiting for transfers between devices  198 us (53%)
  Pallas kernels  79 us (21%)
  matrix products  45.5 us (12%)
  local copies, waits for them, and re-layouts  16.5 us (4%)
  between operations  13.9 us (4%)
  other arithmetic  13.6 us (4%)
  starting transfers between devices  7.02 us (2%)
    reduce_scatter x3, waiting for transfers between devices, scatter_rows(): lax.psum_scatter(value.astype(BF16), 'outer', scatter_dimension=0, tiled=...  93.8 us
    pallas_call x1, Pallas kernels, front(): pl.pallas_call(functools.partial(front_kernel, n_outer, n_tp, conv), name...  79 us
    ppermute x3, waiting for transfers between devices, swap(): return lax.ppermute(value, 'pair', [(0, 1), (1, 0)])  61.3 us
    dot_general x6, matrix products, contract_tokens(): lax.dot_general(left, right, (((1,), (0,)), ((), ())), preferred_element_...  25.9 us
    ppermute x3, waiting for transfers between devices, sum_tokens(): lax.ppermute(value, SP, [(i, i ^ step) for i in range(count)])  24.6 us
    dot_general x2, matrix products, contract_channels(): lax.dot_general(left, right, (((1,), (1,)), ((), ())), preferred_element_...  19.6 us
    ppermute x3, waiting for transfers between devices, scatter_channels(): lax.ppermute(part(me + step), 'tp', [(i, (i + step) % count) for i in ran...  17.7 us
    dynamic_slice x3, local copies, waits for them, and re-layouts, mine(): return lax.dynamic_index_in_dim(split, own, 1, keepdims=False)  10.4 us
  transfers between devices with their start and end apart: 12, of which 9 were waited for; matrix products, arithmetic and copies ran while one was open for 16% of the time, Pallas kernels for 0%

profile of v1, /device:TPU:19, one launch (start us, length us, event | category | flops | bytes accessed | tf_op | source)
XLA Modules:
  0.0 373.2 jit_solution(11779495825655265402)
XLA Ops:
  8.7 79.0 %front.1 = (bf16[8,512,512]{2,1,0:T(8,128)(2,1)}, bf16[8,512,512]{2,1,0:T(8,128)(2,1)}, bf16[4,512,512]{2,1,0:T(8,128)(2,1)}, bf16[4,512,512]{2,1,0:T(8,128)(2,1...) custom-call(bf16[512,1024]{1,0:T(8,128)(2,1)} %x_ref.1, ...), custom_call_target="tpu_custom_call" | custom-call | flops 12884901888 | bytes 41943040 | tf_op jit(solution)/shard_map/front/pallas_call | solution.py:419
  87.9 3.9 %constant_dynamic-slice_fusion = (bf16[4,1,512,512]{3,2,1,0:T(8,128)(2,1)}, bf16[4,1,512,512]{3,2,1,0:T(8,128)(2,1)S(1)}) fusion(bf16[4,2,512,512]{3,2,1,0:T(8,128)(2,1)} %bitcast.70, s32[]{:T(128)S(6)} %select_n.22, bf16[4,2,512,512]{3,2,1,0:T(8,128)(2,1)} %bitcast.69), kind=kLoop, calls=%fused_computation.17 | loop fusion | bytes 8388612 | tf_op jit(solution)/shard_map/jit(dynamic_index_in_dim)/dynamic_slice | solution.py:492
  91.8 4.1 %copy.20 = bf16[4,1,512,512]{2,3,0,1:T(8,128)(2,1)} copy(bf16[4,1,512,512]{3,2,1,0:T(8,128)(2,1)} %get-tuple-element.25) | data formatting | bytes 4194304 | tf_op jit(solution)/shard_map/jit(dynamic_index_in_dim)/dynamic_slice | solution.py:492
  95.9 16.7 %collective-permute-done.5 = bf16[512,1024]{1,0:T(8,128)(2,1)S(1)} collective-permute-done((bf16[512,1024]{1,0:T(8,128)(2,1)}, bf16[512,1024]{1,0:T(8,128)(2,1)S(1)}, u32[]{:S(2)}, u32[]{:S(2)}) %collective-permute-start.5) | collective-permute-done | bytes 1048608 | tf_op jit(solution)/shard_map/ppermute | solution.py:453
  112.6 4.1 %fusion.3 = f32[4,512,1024]{2,1,0:T(8,128)S(1)} fusion(bf16[4,512,512]{2,1,0:T(8,128)(2,1)} %get-tuple-element.20, bf16[512,1024]{1,0:T(8,128)(2,1)S(1)} %collective-permute-done.5), kind=kOutput, calls=%fused_computation.8 | convolution fusion | flops 2147483648 | bytes 11534336 | tf_op jit(solution)/shard_map/dot_general | solution.py:461
  116.8 4.4 %fusion = bf16[2048,1024]{1,0:T(8,128)(2,1)} fusion(f32[4,512,1024]{2,1,0:T(8,128)S(1)} %fusion.3, bf16[2048,512]{1,0:T(8,128)(2,1)S(1)} %bitcast.68, bf16[512,1024]{1,0:T(8,128)(2,1)S(1)} %copy-done.8), kind=kOutput, calls=%fused_computation.1 | convolution fusion | flops 2151677952 | bytes 15728640 | tf_op jit(solution)/shard_map/dot_general | solution.py:461
  124.8 21.5 %collective-permute-done.4 = bf16[512,1024]{1,0:T(8,128)(2,1)} collective-permute-done((bf16[512,1024]{1,0:T(8,128)(2,1)S(1)}, bf16[512,1024]{1,0:T(8,128)(2,1)}, u32[]{:S(2)}, u32[]{:S(2)}) %collective-permute-start.4) | collective-permute-done | bytes 1048608 | tf_op jit(solution)/shard_map/ppermute | solution.py:453
  146.3 4.4 %fusion.5 = f32[4,512,1024]{2,1,0:T(8,128)S(1)} fusion(bf16[4,512,512]{2,1,0:T(8,128)(2,1)} %get-tuple-element.17, bf16[512,1024]{1,0:T(8,128)(2,1)} %collective-permute-done.4), kind=kOutput, calls=%fused_computation.10 | convolution fusion | flops 2147483648 | bytes 11534336 | tf_op jit(solution)/shard_map/dot_general | solution.py:461
  150.7 4.5 %fusion.1 = bf16[2048,1024]{1,0:T(8,128)(2,1)} fusion(f32[4,512,1024]{2,1,0:T(8,128)S(1)} %fusion.5, bf16[2048,512]{1,0:T(8,128)(2,1)S(1)} %bitcast.66, bf16[512,1024]{1,0:T(8,128)(2,1)S(1)} %copy-done.5), kind=kOutput, calls=%fused_computation.3 | convolution fusion | flops 2151677952 | bytes 15728640 | tf_op jit(solution)/shard_map/dot_general | solution.py:461
  155.4 23.1 %collective-permute-done.3 = bf16[512,1024]{1,0:T(8,128)(2,1)S(1)} collective-permute-done((bf16[512,1024]{1,0:T(8,128)(2,1)}, bf16[512,1024]{1,0:T(8,128)(2,1)S(1)}, u32[]{:S(2)}, u32[]{:S(2)}) %collective-permute-start.3) | collective-permute-done | bytes 1048608 | tf_op jit(solution)/shard_map/ppermute | solution.py:453
  178.5 4.0 %fusion.7 = f32[4,512,1024]{2,1,0:T(8,128)S(1)} fusion(bf16[4,512,512]{2,1,0:T(8,128)(2,1)} %get-tuple-element.17, bf16[512,1024]{1,0:T(8,128)(2,1)S(1)} %collective-permute-done.3), kind=kOutput, calls=%fused_computation.12 | convolution fusion | flops 2147483648 | bytes 11534336 | tf_op jit(solution)/shard_map/dot_general | solution.py:461
  182.5 4.5 %fusion.2 = bf16[2048,1024]{1,0:T(8,128)(2,1)} fusion(f32[4,512,1024]{2,1,0:T(8,128)S(1)} %fusion.7, bf16[2048,512]{1,0:T(8,128)(2,1)S(1)} %bitcast.67, bf16[512,1024]{1,0:T(8,128)(2,1)S(1)} %copy-done.6), kind=kOutput, calls=%fused_computation.5 | convolution fusion | flops 2151677952 | bytes 15728640 | tf_op jit(solution)/shard_map/dot_general | solution.py:461
  188.3 10.1 %fusion.10 = f32[512,4096]{1,0:T(8,128)} fusion(bf16[512,1024]{1,0:T(8,128)(2,1)S(1)} %copy-done.7, bf16[4096,1024]{1,0:T(8,128)(2,1)} %wv_ref.1), kind=kOutput, calls=%fused_computation.23 | convolution fusion | flops 4294967296 | bytes 17825792 | tf_op jit(solution)/shard_map/dot_general | solution.py:457
  198.4 9.5 %add_convert_fusion = bf16[512,4096]{1,0:T(8,128)(2,1)S(1)} fusion(f32[512,4096]{1,0:T(8,128)} %fusion.10, bf16[512,1024]{1,0:T(8,128)(2,1)S(1)} %copy-done.5, bf16[4096,1024]{1,0:T(8,128)(2,1)} %wg_ref.1), kind=kOutput, calls=%fused_computation.6 | convolution fusion | flops 4299161600 | bytes 22020096 | tf_op jit(solution)/shard_map/dot_general | solution.py:457
  211.1 2.9 collective-permute-start
  215.2 4.2 %collective-permute-done.6 = f32[32,1024]{1,0:T(8,128)S(1)} collective-permute-done((f32[32,1024]{1,0:T(8,128)S(1)}, f32[32,1024]{1,0:T(8,128)S(1)}, u32[]{:S(2)}, u32[]{:S(2)}) %collective-permute-start.6) | collective-permute-done | bytes 131104 | tf_op jit(solution)/shard_map/ppermute | solution.py:447
  221.2 8.7 %collective-permute-done.7 = f32[32,1024]{1,0:T(8,128)S(1)} collective-permute-done((f32[32,1024]{1,0:T(8,128)S(1)}, f32[32,1024]{1,0:T(8,128)S(1)}, u32[]{:S(2)}, u32[]{:S(2)}) %collective-permute-start.7) | collective-permute-done | bytes 131104 | tf_op jit(solution)/shard_map/ppermute | solution.py:447
  230.7 11.6 %collective-permute-done.8 = f32[32,1024]{1,0:T(8,128)S(1)} collective-permute-done((f32[32,1024]{1,0:T(8,128)S(1)}, f32[32,1024]{1,0:T(8,128)S(1)}, u32[]{:S(2)}, u32[]{:S(2)}) %collective-permute-start.8) | collective-permute-done | bytes 131104 | tf_op jit(solution)/shard_map/ppermute | solution.py:447
  243.0 17.7 %collective-permute-done.1 = bf16[512,1024]{1,0:T(8,128)(2,1)} collective-permute-done((bf16[512,1024]{1,0:T(8,128)(2,1)S(1)}, bf16[512,1024]{1,0:T(8,128)(2,1)}, u32[]{:S(2)}, u32[]{:S(2)}) %collective-permute-start.1) | collective-permute-done | bytes 1048608 | tf_op jit(solution)/shard_map/ppermute | solution.py:478
  260.7 3.7 add_convert_fusion.1
  264.4 2.8 convert_element_type.50
  267.2 17.0 %reduce-scatter.6.cloned.1.call-done = bf16[512,1024]{1,0:T(8,128)(2,1)} async-done(((bf16[2048,1024]{1,0:T(8,128)(2,1)}), bf16[512,1024]{1,0:T(8,128)(2,1)}) %reduce-scatter.6.cloned.1.call-update) | async-done | bytes 1048592 | tf_op jit(solution)/shard_map/reduce_scatter | solution.py:466
  284.2 2.8 convert_element_type.48
  287.0 76.8 %reduce-scatter.4.cloned.1.call-done = bf16[512,1024]{1,0:T(8,128)(2,1)} async-done(((bf16[2048,1024]{1,0:T(8,128)(2,1)}), bf16[512,1024]{1,0:T(8,128)(2,1)}) %reduce-scatter.4.cloned.1.call-update) | async-done | bytes 1048592 | tf_op jit(solution)/shard_map/reduce_scatter | solution.py:466
  (44 shorter events, 16.9 us)
Async XLA Ops:
  7.2 257.3 %reduce-scatter.8.cloned.1.call-start = ((), (), s32[]{:S(2)}) async-start(), calls=%async_computation.5 | async-start | bytes 5242880 | tf_op jit(solution)/shard_map/reduce_scatter | solution.py:466
  87.8 24.9 %collective-permute-start.5 = (bf16[512,1024]{1,0:T(8,128)(2,1)}, bf16[512,1024]{1,0:T(8,128)(2,1)S(1)}, u32[]{:S(2)}, u32[]{:S(2)}) collective-permute-start(bf16[512,1024]{1,0:T(8,128)(2,1)} %get-tuple-element.19), channel_id=1, source_target_pairs={{0,4},{4,0},{1,5},{5,1},{2,6},{6,2},{3,7},{7,3},{8,12},{12,8},{9,1... | collective-permute-start | bytes 3145736 | tf_op jit(solution)/shard_map/ppermute | solution.py:453
  112.6 4.1 %copy-start.2 = (bf16[4,1,512,512]{2,3,0,1:T(8,128)(2,1)S(1)}, bf16[4,1,512,512]{2,3,0,1:T(8,128)(2,1)}, u32[]{:S(2)}) copy-start(bf16[4,1,512,512]{2,3,0,1:T(8,128)(2,1)} %copy.20) | copy-start | bytes 6291460
  112.6 4.1 %copy-start.8 = (bf16[512,1024]{1,0:T(8,128)(2,1)S(1)}, bf16[512,1024]{1,0:T(8,128)(2,1)}, u32[]{:S(2)}) copy-start(bf16[512,1024]{1,0:T(8,128)(2,1)} %get-tuple-element.19) | copy-start | bytes 3145732
  121.2 1.2 copy-start.5
  121.2 163.0 %reduce-scatter.6.cloned.1.call-start = ((), (), s32[]{:S(2)}) async-start(), calls=%async_computation.4 | async-start | bytes 5242880 | tf_op jit(solution)/shard_map/reduce_scatter | solution.py:466
  122.4 23.9 %collective-permute-start.4 = (bf16[512,1024]{1,0:T(8,128)(2,1)S(1)}, bf16[512,1024]{1,0:T(8,128)(2,1)}, u32[]{:S(2)}, u32[]{:S(2)}) collective-permute-start(bf16[512,1024]{1,0:T(8,128)(2,1)S(1)} %copy-done.5), channel_id=1, source_target_pairs={{0,4},{4,0},{1,5},{5,1},{2,6},{6,2},{3,7},{7,3},{8,12},{12,8},{9,1... | collective-permute-start | bytes 3145736 | tf_op jit(solution)/shard_map/ppermute | solution.py:453
  146.3 4.4 %copy-start.1 = (bf16[4,1,512,512]{2,3,0,1:T(8,128)(2,1)S(1)}, bf16[4,1,512,512]{2,3,0,1:T(8,128)(2,1)}, u32[]{:S(2)}) copy-start(bf16[4,1,512,512]{2,3,0,1:T(8,128)(2,1)} %copy.17) | copy-start | bytes 6291460
  155.2 208.6 %reduce-scatter.4.cloned.1.call-start = ((), (), s32[]{:S(2)}) async-start(), calls=%async_computation.3 | async-start | bytes 5242880 | tf_op jit(solution)/shard_map/reduce_scatter | solution.py:466
  155.3 27.2 %copy-start.6 = (bf16[512,1024]{1,0:T(8,128)(2,1)S(1)}, bf16[512,1024]{1,0:T(8,128)(2,1)}, u32[]{:S(2)}) copy-start(bf16[512,1024]{1,0:T(8,128)(2,1)} %get-tuple-element.14) | copy-start | bytes 3145732
  155.3 23.2 %collective-permute-start.3 = (bf16[512,1024]{1,0:T(8,128)(2,1)}, bf16[512,1024]{1,0:T(8,128)(2,1)S(1)}, u32[]{:S(2)}, u32[]{:S(2)}) collective-permute-start(bf16[512,1024]{1,0:T(8,128)(2,1)} %get-tuple-element.14), channel_id=1, source_target_pairs={{0,4},{4,0},{1,5},{5,1},{2,6},{6,2},{3,7},{7,3},{8,12},{12,8},{9,1... | collective-permute-start | bytes 3145736 | tf_op jit(solution)/shard_map/ppermute | solution.py:453
  187.0 1.3 copy-start.7
  207.9 1.9 copy-start
  209.8 5.3 %copy-start.3 = (f32[8,32,128]{2,1,0:T(8,128)S(1)}, f32[8,32,128]{2,1,0:T(8,128)}, u32[]{:S(2)}) copy-start(f32[8,32,128]{2,1,0:T(8,128)} %get-tuple-element.21) | copy-start | bytes 393220
  211.1 31.9 %collective-permute-start = (bf16[512,1024]{1,0:T(8,128)(2,1)}, bf16[512,1024]{1,0:T(8,128)(2,1)S(1)}, u32[]{:S(2)}, u32[]{:S(2)}) collective-permute-start(bf16[512,1024]{1,0:T(8,128)(2,1)} %get-tuple-element.22), channel_id=1, source_target_pairs={{0,1},{1,2},{2,3},{3,0},{4,5},{5,6},{6,7},{7,4},{8,9},{9,10},{10,1... | collective-permute-start | bytes 3145736 | tf_op jit(solution)/shard_map/ppermute | solution.py:478
  214.1 28.9 %collective-permute-start.2 = (bf16[512,1024]{1,0:T(8,128)(2,1)S(1)}, bf16[512,1024]{1,0:T(8,128)(2,1)}, u32[]{:S(2)}, u32[]{:S(2)}) collective-permute-start(bf16[512,1024]{1,0:T(8,128)(2,1)S(1)} %get-tuple-element.23), channel_id=1, source_target_pairs={{0,3},{1,0},{2,1},{3,2},{4,7},{5,4},{6,5},{7,6},{8,11},{9,8},{10,9... | collective-permute-start | bytes 3145736 | tf_op jit(solution)/shard_map/ppermute | solution.py:478
  214.1 46.6 %collective-permute-start.1 = (bf16[512,1024]{1,0:T(8,128)(2,1)S(1)}, bf16[512,1024]{1,0:T(8,128)(2,1)}, u32[]{:S(2)}, u32[]{:S(2)}) collective-permute-start(bf16[512,1024]{1,0:T(8,128)(2,1)S(1)} %get-tuple-element.24), channel_id=1, source_target_pairs={{0,2},{1,3},{2,0},{3,1},{4,6},{5,7},{6,4},{7,5},{8,10},{9,11},{10,... | collective-permute-start | bytes 3145736 | tf_op jit(solution)/shard_map/ppermute | solution.py:478
  215.1 4.3 %collective-permute-start.6 = (f32[32,1024]{1,0:T(8,128)S(1)}, f32[32,1024]{1,0:T(8,128)S(1)}, u32[]{:S(2)}, u32[]{:S(2)}) collective-permute-start(f32[32,1024]{1,0:T(8,128)S(1)} %copy_bitcast_fusion), channel_id=1, source_target_pairs={{0,4},{4,0},{8,12},{12,8},{16,20},{20,16},{24,28},{28,24},{1,5},{5... | collective-permute-start | bytes 393224 | tf_op jit(solution)/shard_map/ppermute | solution.py:447
  219.4 10.5 %collective-permute-start.7 = (f32[32,1024]{1,0:T(8,128)S(1)}, f32[32,1024]{1,0:T(8,128)S(1)}, u32[]{:S(2)}, u32[]{:S(2)}) collective-permute-start(f32[32,1024]{1,0:T(8,128)S(1)} %fusion.9), channel_id=1, source_target_pairs={{0,8},{4,12},{8,0},{12,4},{16,24},{20,28},{24,16},{28,20},{1,9},{5... | collective-permute-start | bytes 393224 | tf_op jit(solution)/shard_map/ppermute | solution.py:447
  229.9 12.4 %collective-permute-start.8 = (f32[32,1024]{1,0:T(8,128)S(1)}, f32[32,1024]{1,0:T(8,128)S(1)}, u32[]{:S(2)}, u32[]{:S(2)}) collective-permute-start(f32[32,1024]{1,0:T(8,128)S(1)} %add.81), channel_id=1, source_target_pairs={{0,16},{4,20},{8,24},{12,28},{16,0},{20,4},{24,8},{28,12},{1,17},{... | collective-permute-start | bytes 393224 | tf_op jit(solution)/shard_map/ppermute | solution.py:447
  242.3 24.9 %copy-start.4 = (f32[32,1024]{1,0:T(8,128)}, f32[32,1024]{1,0:T(8,128)S(1)}, u32[]{:S(2)}) copy-start(f32[32,1024]{1,0:T(8,128)S(1)} %add.82) | copy-start | bytes 393220
Sparse Core Ops, SparseCore 0:
  121.4 77.6 reduce-scatter.7
  201.3 82.8 reduce-scatter.5
  286.5 77.2 reduce-scatter.3

commit v2 on v1

--- a/solution.py
+++ b/solution.py
@@ -59,10 +59,10 @@
 def front_kernel(
     n_outer, n_tp, conv,
     x_ref, g_ref, wv_ref, wg_ref, wo_ref, taps_ref, gain_ref,
-    xg_out, gg_out, px_out, pg_out, act_out, gv_out, gt_out, small_out,
+    xg_out, gg_out, px_out, pg_out, lg_out, act_out, gv_out, gt_out, small_out,
     xg, gg, wv, wg, wo, pv, ps, ga, cv, hp, gc, act, gv, gt, small,
     sum_a, sum_b, mean_b, inv_b, stat1, stat2,
-    send_sems, recv_x, recv_g, recv_px, recv_pg, recv_h, recv_c, recv_s1, recv_s2, load_sems, own_sems, out_sems,
+    send_sems, recv_x, recv_g, recv_px, recv_pg, recv_l, recv_h, recv_c, recv_s1, recv_s2, load_sems, own_sems, out_sems,
 ):
     outer, pair, tp = (lax.axis_index(name) for name in AXES)
     seq, n_seq, per = outer * 2 + pair, n_outer * 2, (n_outer * 2) // n_tp
@@ -88,6 +88,10 @@
     pl.when(has_before)(lambda: greet(beside(before)))
     pl.when(has_after)(lambda: greet(beside(after)))
     greet(facing)
+    level = lambda index: (index, pair, tp)
+    planes = [lax.rem(outer + step, n_outer) for step in range(1, n_outer)]
+    for other in planes:
+        greet(level(other))
 
     block = lambda b, h: b * per + h
     order = [tp, sibling]
@@ -125,7 +129,7 @@
     for step in range(2 * per, n_tp * per):
         loads[2][step].start()
 
-    count = n_tp - 1 + 1 + has_before.astype(jnp.int32) + has_after.astype(jnp.int32)
+    count = n_tp - 1 + 1 + n_outer - 1 + has_before.astype(jnp.int32) + has_after.astype(jnp.int32)
     pl.semaphore_wait(barrier, count)
 
     sends = Sends(send_sems)
@@ -199,6 +203,9 @@
             ready([twin], (0, 1))
             project([twin], xg, ((wv, pv), (wg, ps)), False)
 
+    for other in planes:
+        sends.start(xg.at[other * 2 + core], lg_out.at[outer, core], recv_l.at[outer, core], level(other))
+
     def gate(i, carry):
         c, r = lax.div(i, tokens // ROWS), lax.rem(i, tokens // ROWS)
         rows = pl.ds(pl.multiple_of(r * ROWS, ROWS), ROWS)
@@ -367,6 +374,14 @@
     for copy in outs[1:]:
         copy.start()
 
+    for other in planes:
+        arrived(lg_out.at[other, core], recv_l.at[other, core])
+        sends.start(lg_out.at[other, core], lg_out.at[other, core], recv_l.at[other, core], home(sibling))
+    own_lefts = [pltpu.make_async_copy(xg.at[outer * 2 + h], lg_out.at[outer, h], out_sems.at[6 + h]) for h in range(2)]
+    for copy in own_lefts:
+        copy.start()
+    outs += own_lefts
+
     mine = [tp] + across
     for crossed, recv in ((px_out, recv_px), (pg_out, recv_pg)):
         for b in mine:
@@ -391,6 +406,8 @@
         for b in mine:
             twin = b + 1 - 2 * core
             arrived(crossed.at[twin], recv.at[twin])
+    for other in planes:
+        arrived(lg_out.at[other, 1 - core], recv_l.at[other, 1 - core])
     sends.drain()
     for copy in outs:
         copy.wait()
@@ -405,13 +422,13 @@
     per, n_lane, n_y = n_seq // n_tp, channels // LANES, n_tp // 2
     tap_cells = jnp.pad(taps.astype(F32), ((0, 1), (0, 0))).reshape(conv + 1, n_lane, LANES).transpose(1, 0, 2)
     gain_cells = ln_gain.reshape(n_lane, 1, LANES)
-    n_sends = 2 * (per * n_y + 1 + (n_y - 1) * per * 2 + n_y) + 4 + 2 * (n_tp - 1)
+    n_sends = 2 * (per * n_y + 1 + (n_y - 1) * per * 2 + n_y) + 4 + 2 * (n_tp - 1) + 2 * (n_outer - 1)
     any_spec, vmem_spec = pl.BlockSpec(memory_space=pl.ANY), pl.BlockSpec(memory_space=pltpu.VMEM)
     lanes = lambda rows, dtype=F32: pltpu.VMEM((n_lane, rows, LANES), dtype)
     dma = lambda *shape: pltpu.SemaphoreType.DMA(shape)
     out_shapes = [
         ((n_seq, tokens, width), BF16), ((n_seq, tokens, width), BF16),
-        ((n_tp, tokens, width), BF16), ((n_tp, tokens, width), BF16),
+        ((n_tp, tokens, width), BF16), ((n_tp, tokens, width), BF16), ((n_outer, 2, tokens, width), BF16),
         ((tokens, channels), BF16), ((tokens, channels), BF16), ((tokens, channels), BF16),
         ((n_lane, conv + 1, LANES), F32),
     ]
@@ -431,8 +448,8 @@
             lanes(conv + 1),
             *[pltpu.VMEM((tokens, LANES), F32)] * 4,
             *[pltpu.VMEM((n_tp, 8, tokens), F32)] * 2,
-            dma(n_sends), dma(n_seq), dma(n_seq), dma(n_tp), dma(n_tp), dma(2), dma(2), dma(n_tp), dma(n_tp),
-            dma(3, n_seq), dma(2, per), dma(6),
+            dma(n_sends), dma(n_seq), dma(n_seq), dma(n_tp), dma(n_tp), dma(n_outer, 2), dma(2), dma(2), dma(n_tp), dma(n_tp),
+            dma(3, n_seq), dma(2, per), dma(8),
         ],
         compiler_params=pltpu.CompilerParams(
             collective_id=0, has_side_effects=True, vmem_limit_bytes=63 * 1024 * 1024
@@ -441,66 +458,357 @@
     )(inputs, grad_out, w_value, w_gate, w_out, tap_cells, gain_cells)
 
 
-def sum_tokens(value):
-    count, step = lax.axis_size(SP), 1
-    while step < count:
-        value = value + lax.ppermute(value, SP, [(i, i ^ step) for i in range(count)])
-        step *= 2
-    return value
-
-
-def swap(value):
-    return lax.ppermute(value, "pair", [(0, 1), (1, 0)])
-
-
-def contract_channels(left, right):
+JOBS = 3
+
+
+def dot_tokens(left, right):
+    return lax.dot_general(left, right, (((0,), (0,)), ((), ())), preferred_element_type=F32)
+
+
+def dot_channels(left, right):
     return lax.dot_general(left, right, (((1,), (1,)), ((), ())), preferred_element_type=F32)
 
 
-def contract_tokens(left, right):
-    value = lax.dot_general(left, right, (((1,), (0,)), ((), ())), preferred_element_type=F32)
-    return value.reshape(-1, value.shape[-1])
-
-
-def scatter_rows(value):
-    return lax.psum_scatter(value.astype(BF16), "outer", scatter_dimension=0, tiled=True).astype(F32)
-
-
-def scatter_channels(value):
-    count, me = lax.axis_size("tp"), lax.axis_index("tp")
-    width = value.shape[1] // count
-
-    def part(owner):
-        return lax.dynamic_slice_in_dim(value, lax.rem(owner, count) * width, width, axis=1)
-
-    total = part(me).astype(F32)
-    for step in range(1, count):
-        sent = lax.ppermute(part(me + step), "tp", [(i, (i + step) % count) for i in range(count)])
-        total = total + sent.astype(F32)
-    return total.astype(BF16)
+def loop(count, body):
+    def step(index, carry):
+        body(index)
+        return carry
+
+    lax.fori_loop(0, count, step, 0)
+
+
+def back_kernel(
+    n_outer, n_tp,
+    act_ref, gv_ref, gt_ref, xg_ref, gg_ref, px_ref, pg_ref, lg_ref, wv_ref, wg_ref, small_ref,
+    gi_out, gvw_out, ggw_out, gow_out, small_out,
+    own_left, pair_left, line_left, ag, rs, own_right, pair_right, gv, gt, weights, gi, gi_sent, gi_total,
+    racc, aacc, xacc, xs, xr, small, small_x, group, group_in, group_all, small_total,
+    load_sems, left_sems, weight_sems, out_sems,
+    ag_send, ag_recv, rs_send, rs_recv, xr_send, xr_recv, swap_send, swap_recv, gi_send, gi_recv,
+    sx_send, sx_recv, s1_send, s1_recv, s2_send, s2_recv,
+):
+    z, pair, tp = (lax.axis_index(name) for name in AXES)
+    n, last = n_outer, n_outer - 1
+    mirror = last - z
+    width, half = own_left.shape[3], own_right.shape[2]
+    per = gi.shape[1]
+    facing = (z, 1 - pair, tp)
+    level = lambda index: (index, pair, tp)
+    home = lambda index: (z, pair, index)
+
+    barrier = pltpu.get_barrier_semaphore()
+
+    def greet(device):
+        pl.semaphore_signal(barrier, inc=1, device_id=device, device_id_type=MESH)
+
+    greet(facing)
+    for step in range(1, n):
+        greet(level(lax.rem(z + step, n)))
+    for step in range(1, n_tp):
+        greet(home(lax.rem(tp + step, n_tp)))
+
+    def remote(src, dst, send, recv, device):
+        return pltpu.make_async_remote_copy(
+            src_ref=src, dst_ref=dst, send_sem=send, recv_sem=recv, device_id=device, device_id_type=MESH
+        )
+
+    local = []
+
+    def load(src, dst, sem):
+        copy = pltpu.make_async_copy(src, dst, sem)
+        copy.start()
+        return copy
+
+    def weight_copies(s, slot):
+        b, h = lax.rem(tp + 1 + lax.div(s, per), n_tp), lax.rem(s, per)
+        row = pl.multiple_of((b * per + h) * width, width)
+        return [
+            pltpu.make_async_copy(ref.at[pl.ds(row, width), :], weights.at[slot, i], weight_sems.at[slot, i])
+            for i, ref in enumerate((wv_ref, wg_ref))
+        ]
+
+    lead, trail = pl.ds(0, half), pl.ds(half, half)
+    cells = [
+        load(gv_ref.at[:, trail], ag.at[0, z], load_sems.at[0]),
+        load(gt_ref.at[:, lead], ag.at[1, z], load_sems.at[1]),
+        load(gt_ref.at[:, trail], ag.at[2, z], load_sems.at[2]),
+    ]
+    whole = [load(gv_ref, gv, load_sems.at[3]), load(gt_ref, gt, load_sems.at[4])]
+    for copy in weight_copies(0, 0):
+        copy.start()
+    rights = [
+        load(act_ref.at[:, lead], own_right.at[0], load_sems.at[5]),
+        load(act_ref.at[:, trail], own_right.at[1], load_sems.at[6]),
+        load(gv_ref.at[:, lead], own_right.at[2], load_sems.at[7]),
+        load(small_ref, small, load_sems.at[8]),
+    ]
+    lefts = []
+    for d in range(n):
+        lefts += [
+            load(gg_ref.at[d * 2 + pair], own_left.at[0, d], left_sems.at[0, d]),
+            load(xg_ref.at[d * 2 + pair], own_left.at[1, d], left_sems.at[1, d]),
+            load(pg_ref.at[d], pair_left.at[0, d], left_sems.at[2, d]),
+            load(px_ref.at[d], pair_left.at[1, d], left_sems.at[3, d]),
+            load(lg_ref.at[d], line_left.at[d], left_sems.at[4, d]),
+        ]
+
+    pl.semaphore_wait(barrier, 1 + n - 1 + n_tp - 1)
+
+    for copy in cells:
+        copy.wait()
+
+    def ag_right(k, j):
+        return remote(ag.at[j, z - k], ag.at[j, z - k], ag_send.at[0, j, k], ag_recv.at[j, z - k], level(z + 1))
+
+    def ag_left(k, j):
+        return remote(ag.at[j, z + k], ag.at[j, z + k], ag_send.at[1, j, k], ag_recv.at[j, z + k], level(z - 1))
+
+    for j in range(JOBS):
+        pl.when(z < last)(lambda: ag_right(0, j).start())
+        pl.when(z > 0)(lambda: ag_left(0, j).start())
+    swaps = [
+        remote(src, pair_right.at[j], swap_send.at[j], swap_recv.at[j], facing)
+        for j, src in enumerate((act_ref.at[:, lead], act_ref.at[:, trail], gv_ref.at[:, lead]))
+    ]
+    small_swap = remote(small_ref, small_x, sx_send.at[0], sx_recv.at[0], facing)
+    small_swap.start()
+    for copy in swaps:
+        copy.start()
+
+    for copy in whole:
+        copy.wait()
+    steps = n_tp * per
+
+    def input_step(s):
+        slot = lax.rem(s, 2)
+
+        @pl.when(s < steps - 1)
+        def _():
+            for copy in weight_copies(s + 1, 1 - slot):
+                copy.start()
+
+        for copy in weight_copies(s, slot):
+            copy.wait()
+        b, h = lax.rem(tp + 1 + lax.div(s, per), n_tp), lax.rem(s, per)
+        value = (dot_channels(gv[...], weights[slot, 0]) + dot_channels(gt[...], weights[slot, 1])).astype(BF16)
+
+        @pl.when(s < steps - per)
+        def _():
+            gi_sent[s] = value
+            remote(gi_sent.at[s], gi.at[tp, h], gi_send.at[s], gi_recv.at[tp, h], home(b)).start()
+
+        @pl.when(s >= steps - per)
+        def _():
+            gi[tp, h] = value
+
+    loop(steps, input_step)
+
+    for copy in rights:
+        copy.wait()
+    small_swap.wait_recv()
+    rows = group.shape[2]
+    for g in range(n):
+        group[g] = small[:, g * rows : (g + 1) * rows, :] + small_x[:, g * rows : (g + 1) * rows, :]
+    group_in[z] = group[z]
+    for step in range(1, n):
+        other = lax.rem(z + step, n)
+        remote(group.at[other], group_in.at[z], s1_send.at[step], s1_recv.at[z], level(other)).start()
+    for copy in lefts:
+        copy.wait()
+    for copy in swaps:
+        copy.wait_recv()
+
+    def partial_rows(j, d):
+        tensor = lax.div(j, 2)
+        return dot_tokens(own_left[tensor, d], own_right[j]) + dot_tokens(pair_left[tensor, d], pair_right[j])
+
+    def own_rows(j):
+        racc[j] = partial_rows(j, z)
+
+    def line_rows(j, source, first):
+        cells = ag[j, source]
+        mine = dot_tokens(line_left[source, pair], cells)
+        theirs = dot_tokens(line_left[source, 1 - pair], cells)
+        if first:
+            aacc[j], xacc[j] = mine, theirs
+        else:
+            aacc[j] += mine
+            xacc[j] += theirs
+
+    def rs_right(j, d):
+        return remote(rs.at[j, d], rs.at[j, d], rs_send.at[j, d], rs_recv.at[j, d], level(z + 1))
+
+    def rs_left(j, d):
+        slot = jnp.where(d == z - 1, n, d)
+        return remote(rs.at[j, d], rs.at[j, slot], rs_send.at[j, d], rs_recv.at[j, slot], level(z - 1))
+
+    def reduce_step(j, d, waiting, copy):
+        value = partial_rows(j, d)
+
+        @pl.when(waiting)
+        def _():
+            arrived(rs.at[j, d], rs_recv.at[j, d])
+            rs[j, d] = (value + rs[j, d].astype(F32)).astype(BF16)
+
+        @pl.when(jnp.logical_not(waiting))
+        def _():
+            rs[j, d] = value.astype(BF16)
+
+        copy(j, d).start()
+
+    farthest = jnp.maximum(z, mirror)
+
+    def cross(j):
+        xs[j] = xacc[j].astype(BF16)
+        remote(xs.at[j], xr.at[j], xr_send.at[j], xr_recv.at[j], facing).start()
+
+    loop(JOBS, lambda j: line_rows(j, z, True))
+
+    def period(index):
+        k = index + 1
+
+        def job(j):
+            @pl.when(k <= z)
+            def _():
+                arrived(ag.at[j, z - k], ag_recv.at[j, z - k])
+                pl.when(z < last)(lambda: ag_right(k, j).start())
+
+            @pl.when(k <= mirror)
+            def _():
+                arrived(ag.at[j, z + k], ag_recv.at[j, z + k])
+                pl.when(z > 0)(lambda: ag_left(k, j).start())
+
+            @pl.when(jnp.logical_and(z < last, k > z))
+            def _():
+                reduce_step(j, n + z - k, z > 0, rs_right)
+
+            @pl.when(jnp.logical_and(z > 0, k > mirror))
+            def _():
+                reduce_step(j, k - mirror - 1, z < last, rs_left)
+
+            pl.when(k <= z)(lambda: line_rows(j, z - k, False))
+            pl.when(k <= mirror)(lambda: line_rows(j, z + k, False))
+            pl.when(k == farthest)(lambda: cross(j))
+
+        loop(JOBS, job)
+
+        @pl.when(index == 0)
+        def _():
+            for step in range(1, n):
+                other = lax.rem(z + step, n)
+                arrived(group_in.at[other], s1_recv.at[other])
+            total = group_in[0]
+            for other in range(1, n):
+                total = total + group_in[other]
+            group_all[z] = total
+            for step in range(1, n):
+                remote(group_all.at[z], group_all.at[z], s2_send.at[step], s2_recv.at[z], level(lax.rem(z + step, n))).start()
+            loop(JOBS, own_rows)
+
+    loop(last, period)
+
+    for step in range(1, n_tp):
+        other = lax.rem(tp + step, n_tp)
+        for h in range(per):
+            arrived(gi.at[other, h], gi_recv.at[other, h])
+    for h in range(per):
+        total = gi[0, h].astype(F32)
+        for other in range(1, n_tp):
+            total = total + gi[other, h].astype(F32)
+        gi_total[:, h * width : (h + 1) * width] = total.astype(BF16)
+    outs = [load(gi_total, gi_out, out_sems.at[0])]
+    for step in range(1, n):
+        other = lax.rem(z + step, n)
+        arrived(group_all.at[other], s2_recv.at[other])
+    for g in range(n):
+        for c in range(small.shape[0]):
+            small_total[g * rows : (g + 1) * rows, c * LANES : (c + 1) * LANES] = group_all[g, c]
+    outs.append(load(small_total, small_out, out_sems.at[1]))
+
+    results = ((gvw_out, trail), (ggw_out, lead), (ggw_out, trail))
+    for j, (ref, columns) in enumerate(results):
+        arrived(xr.at[j], xr_recv.at[j])
+        aacc[j] += xr[j].astype(F32)
+        outs.append(load(aacc.at[j], ref.at[:, columns], out_sems.at[2 + j]))
+    results = ((gow_out, lead), (gow_out, trail), (gvw_out, lead))
+    for j, (ref, columns) in enumerate(results):
+        @pl.when(z > 0)
+        def _():
+            arrived(rs.at[j, z], rs_recv.at[j, z])
+            racc[j] += rs[j, z].astype(F32)
+
+        @pl.when(z < last)
+        def _():
+            arrived(rs.at[j, n], rs_recv.at[j, n])
+            racc[j] += rs[j, n].astype(F32)
+
+        outs.append(load(racc.at[j], ref.at[:, columns], out_sems.at[5 + j]))
+
+    def sent(j):
+        def step(k):
+            pl.when(jnp.logical_and(k <= z, z < last))(lambda: ag_right(k, j).wait_send())
+            pl.when(jnp.logical_and(k <= mirror, z > 0))(lambda: ag_left(k, j).wait_send())
+            pl.when(k > z)(lambda: rs_right(j, k).wait_send())
+            pl.when(k < z)(lambda: rs_left(j, k).wait_send())
+
+        loop(n, step)
+        remote(xs.at[j], xr.at[j], xr_send.at[j], xr_recv.at[j], facing).wait_send()
+
+    loop(JOBS, sent)
+    for copy in swaps + [small_swap]:
+        copy.wait_send()
+    loop(steps - per, lambda s: remote(gi_sent.at[s], gi.at[tp, 0], gi_send.at[s], gi_recv.at[tp, 0], facing).wait_send())
+    for step in range(1, n):
+        remote(group.at[0], group_in.at[z], s1_send.at[step], s1_recv.at[z], facing).wait_send()
+        remote(group_all.at[z], group_all.at[z], s2_send.at[step], s2_recv.at[z], facing).wait_send()
+    for copy in outs:
+        copy.wait()
+
+
+def back(act, gv, gt, xg, gg, px, pg, lg, w_value, w_gate, small):
+    n, n_tp = lax.axis_size("outer"), lax.axis_size("tp")
+    n_seq, tokens, width = xg.shape
+    channels = act.shape[1]
+    n_lane, n_small = small.shape[:2]
+    per, half, rows = n_seq // n_tp, channels // 2, n_small // n
+    any_spec = pl.BlockSpec(memory_space=pl.ANY)
+    dma = lambda *shape: pltpu.SemaphoreType.DMA(shape)
+    bf, wide = (lambda *shape: pltpu.VMEM(shape, BF16)), (lambda *shape: pltpu.VMEM(shape, F32))
+    out_shapes = [((tokens, width * per), BF16)] + [((width, channels), F32)] * 3 + [((n_small, channels), F32)]
+    flops = 2 * 5 * tokens * width * n_seq * channels
+    return pl.pallas_call(
+        functools.partial(back_kernel, n, n_tp),
+        name="back",
+        out_shape=[jax.ShapeDtypeStruct(shape, dtype) for shape, dtype in out_shapes],
+        in_specs=[any_spec] * 11,
+        out_specs=[any_spec] * len(out_shapes),
+        scratch_shapes=[
+            bf(2, n, tokens, width), bf(2, n, tokens, width), bf(n, 2, tokens, width),
+            bf(JOBS, n, tokens, half), bf(JOBS, n + 1, width, half), bf(JOBS, tokens, half), bf(JOBS, tokens, half),
+            bf(tokens, channels), bf(tokens, channels), bf(2, 2, width, channels),
+            bf(n_tp, per, tokens, width), bf((n_tp - 1) * per, tokens, width), bf(tokens, width * per),
+            wide(JOBS, width, half), wide(JOBS, width, half), wide(JOBS, width, half),
+            bf(JOBS, width, half), bf(JOBS, width, half),
+            wide(n_lane, n_small, LANES), wide(n_lane, n_small, LANES),
+            *[wide(n, n_lane, rows, LANES)] * 3, wide(n_small, channels),
+            dma(9), dma(5, n), dma(2, 2), dma(8),
+            dma(2, JOBS, n), dma(JOBS, n), dma(JOBS, n + 1), dma(JOBS, n + 1), dma(JOBS), dma(JOBS), dma(JOBS), dma(JOBS),
+            dma((n_tp - 1) * per), dma(n_tp, per),
+            dma(1), dma(1), dma(n), dma(n), dma(n), dma(n),
+        ],
+        compiler_params=pltpu.CompilerParams(
+            collective_id=1, has_side_effects=True, vmem_limit_bytes=63 * 1024 * 1024
+        ),
+        cost_estimate=pl.CostEstimate(flops=flops, bytes_accessed=60 * 2**20, transcendentals=0),
+    )(act, gv, gt, xg, gg, px, pg, lg, w_value, w_gate, small)
 
 
 def local(inputs, w_value, w_gate, taps, ln_gain, w_out, grad_out):
-    xg, gg, px, pg, activated, grad_value, grad_gate, small = front(
-        inputs, w_value, w_gate, taps, ln_gain, w_out, grad_out
+    xg, gg, px, pg, lg, act, gv, gt, small = front(inputs, w_value, w_gate, taps, ln_gain, w_out, grad_out)
+    grad_input, grad_value_w, grad_gate_w, grad_out_w, token_sums = back(
+        act, gv, gt, xg, gg, px, pg, lg, w_value, w_gate, small
     )
-    own = lax.axis_index("pair")
-    conv = taps.shape[0]
-
-    def mine(cells):
-        split = cells.reshape(cells.shape[0] // 2, 2, *cells.shape[1:])
-        return lax.dynamic_index_in_dim(split, own, 1, keepdims=False)
-
-    pair_activated = swap(activated)
-    pair_value, pair_gate = swap(grad_value), swap(grad_gate)
-    token_sums = sum_tokens(small.transpose(1, 0, 2).reshape(conv + 1, -1))
-    grad_taps, grad_gain = token_sums[:-1], token_sums[-1]
-    grad_out_w = scatter_rows(contract_tokens(mine(gg), activated) + contract_tokens(pg, pair_activated))
-    grad_value_w = scatter_rows(contract_tokens(mine(xg), grad_value) + contract_tokens(px, pair_value))
-    grad_gate_w = scatter_rows(contract_tokens(mine(xg), grad_gate) + contract_tokens(px, pair_gate))
-    partial_value = contract_channels(grad_value, w_value) + contract_channels(grad_gate, w_gate)
-    grad_input = scatter_channels(partial_value.astype(BF16))
-    return (grad_input, grad_value_w, grad_gate_w, grad_out_w, grad_taps, grad_gain)
+    return (grad_input, grad_value_w, grad_gate_w, grad_out_w, token_sums[:-1], token_sums[-1])
 
 
 def solution(mesh):

time: 375 us -> 282 us (0.75)
  waiting for transfers between devices: 198 us -> 0 us
  Pallas kernels: 79 us -> 264 us
  matrix products: 45.5 us -> 0 us
  between operations: 13.9 us -> 0.66 us
  other arithmetic: 13.6 us -> 1.5 us
  starting transfers between devices: 7.02 us -> 0 us
  local copies, waits for them, and re-layouts: 16.5 us -> 10.4 us
    pallas_call x0 -> x1, Pallas kernels: none -> 149 us  [back(): pl.pallas_call(functools.partial(back_kernel, n, n_tp), name='back', out_...]
    ppermute x9 -> x0, waiting for transfers between devices: 104 us -> none  [the longest x3 61.3 us: swap(): return lax.ppermute(value, 'pair', [(0, 1), (1, 0)])]
    reduce_scatter x3 -> x0, waiting for transfers between devices: 93.8 us -> none  [scatter_rows(): lax.psum_scatter(value.astype(BF16), 'outer', scatter_dimension=0, tiled=...]
    dot_general x8 -> x0, matrix products: 45.5 us -> none  [the longest x6 25.9 us: contract_tokens(): lax.dot_general(left, right, (((1,), (0,)), ((), ())), preferred_element_...]
    pallas_call x1, Pallas kernels: 79 us -> 115 us  [front(): pl.pallas_call(functools.partial(front_kernel, n_outer, n_tp, conv), name...]
    convert_element_type x4 -> x0, other arithmetic: 12.1 us -> none  [the longest x3 8.37 us: scatter_rows(): lax.psum_scatter(value.astype(BF16), 'outer', scatter_dimension=0, tiled=...]
    dynamic_slice x4 -> x0, local copies, waits for them, and re-layouts: 11.7 us -> none  [the longest x3 10.4 us: mine(): return lax.dynamic_index_in_dim(split, own, 1, keepdims=False)]
    ppermute x9 -> x0, starting transfers between devices: 6.72 us -> none  [the longest x3 3.93 us: scatter_channels(): lax.ppermute(part(me + step), 'tp', [(i, (i + step) % count) for i in ran...]
  transfers between devices with their start and end apart: 12 -> 0, of which waited for: 9 -> 0; matrix products, arithmetic and copies ran while one was open for 16% -> 0% of each run, Pallas kernels for 0% -> 0%
where the time goes in v2:
time: 282 us; the launch traced here: 277 us
  Pallas kernels  264 us (94%)
  local copies, waits for them, and re-layouts  10.4 us (4%)
    pallas_call x1, Pallas kernels, back(): pl.pallas_call(functools.partial(back_kernel, n, n_tp), name='back', out_...  149 us
    pallas_call x1, Pallas kernels, front(): pl.pallas_call(functools.partial(front_kernel, n_outer, n_tp, conv), name...  115 us
    unnamed x13, local copies, waits for them, and re-layouts  8.94 us

profile of v2, /device:TPU:19, one launch (start us, length us, event | category | flops | bytes accessed | tf_op | source)
XLA Modules:
  0.0 276.6 jit_solution(16652229539583540448)
XLA Ops:
  0.6 1.5 bitcast_bitcast_fusion.taps_ref
  2.1 114.6 %front.1 = (bf16[8,512,512]{2,1,0:T(8,128)(2,1)}, bf16[8,512,512]{2,1,0:T(8,128)(2,1)}, bf16[4,512,512]{2,1,0:T(8,128)(2,1)}, bf16[4,512,512]{2,1,0:T(8,128)(2,1...) custom-call(bf16[512,1024]{1,0:T(8,128)(2,1)} %x_ref.1, ...), custom_call_target="tpu_custom_call" | custom-call | flops 12884901888 | bytes 41943040 | tf_op jit(solution)/shard_map/front/pallas_call | solution.py:436
  116.8 149.3 %back.1 = (bf16[512,1024]{1,0:T(8,128)(2,1)}, f32[512,1024]{1,0:T(8,128)}, f32[512,1024]{1,0:T(8,128)}, f32[512,1024]{1,0:T(8,128)}, f32[32,1024]{1,0:T(8,128)}) custom-call(bf16[512,1024]{1,0:T(8,128)(2,1)} %get-tuple-element.20.act_ref, bf16[512,1024]{1,0:T(8,128)(2,1)} %get-tuple-element.21.gv_ref, bf16[512,1024]{1,0:T(8,128)(2,1)} %get-tuple-element.22.gt_ref, ...), custom_call_target="tpu_custom_call" | custom-call | flops 21474836480 | bytes 62914560 | tf_op jit(solution)/shard_map/back/pallas_call | solution.py:779
  266.1 0.0 copy-start.2
  266.1 1.5 slice.7
  267.7 2.3 copy.21
  269.9 0.0 copy-done.2
  269.9 0.0 copy-start.1
  269.9 1.3 copy.22
  271.2 1.0 copy-done.1
  272.3 0.0 copy-start
  272.3 1.3 copy.23
  273.6 1.0 copy-done
  274.6 0.0 copy-start.3
  274.6 1.3 copy.24
  275.9 0.0 copy-done.3
  275.9 0.7 copy.25
Async XLA Ops:
  266.1 3.8 %copy-start.2 = (f32[512,1024]{1,0:T(8,128)S(1)}, f32[512,1024]{1,0:T(8,128)}, u32[]{:S(2)}) copy-start(f32[512,1024]{1,0:T(8,128)} %get-tuple-element.41) | copy-start | bytes 6291460
  269.9 2.3 copy-start.1
  272.3 2.3 copy-start
  274.6 1.3 copy-start.3

commit v3 on v2

--- a/solution.py
+++ b/solution.py
@@ -59,7 +59,7 @@
 def front_kernel(
     n_outer, n_tp, conv,
     x_ref, g_ref, wv_ref, wg_ref, wo_ref, taps_ref, gain_ref,
-    xg_out, gg_out, px_out, pg_out, lg_out, act_out, gv_out, gt_out, small_out,
+    xg_out, gg_out, px_out, pg_out, lg_out, act_out, gv_out, gt_out, small_out, hp_out, gc_out,
     xg, gg, wv, wg, wo, pv, ps, ga, cv, hp, gc, act, gv, gt, small,
     sum_a, sum_b, mean_b, inv_b, stat1, stat2,
     send_sems, recv_x, recv_g, recv_px, recv_pg, recv_l, recv_h, recv_c, recv_s1, recv_s2, load_sems, own_sems, out_sems,
@@ -142,6 +142,17 @@
     sends.start(x_ref.at[:, pl.ds(crossing, width)], px_out.at[tp], recv_px.at[tp], facing)
     sends.start(g_ref.at[:, pl.ds(crossing, width)], pg_out.at[tp], recv_pg.at[tp], facing)
 
+    part, n_part = lax.div(tp, 2), tokens // n_y
+    part_rows = lambda index: pl.ds(pl.multiple_of(index * n_part, n_part), n_part)
+
+    def line_send(src, b, cond):
+        sends.start_if(
+            jnp.logical_and(cond, b != outer), src, lg_out.at[outer, core, part_rows(part)],
+            recv_l.at[outer, core, part], level(b),
+        )
+
+    line_send(x_ref.at[part_rows(part), pl.ds(pl.multiple_of(core * width, width), width)], tp, True)
+
     def project(ranks, left, pairs, first):
         def body(j, carry):
             column = pl.multiple_of(j * 256, 256)
@@ -176,6 +187,7 @@
     for rank in side:
         index = block(sibling, rank % per)
         arrived(xg.at[index], recv_x.at[index])
+    line_send(xg.at[block(sibling, core), part_rows(part)], sibling, True)
     ready(side, (0, 1))
     project(side, xg, ((wv, pv), (wg, ps)), False)
     for copy in owns[1]:
@@ -195,16 +207,15 @@
     for step, other in enumerate(across):
         for h in range(per):
             land(xg, recv_x, other, h, px_out, recv_px)
+            line_send(xg.at[block(other, h), part_rows(part)], other, core == h)
             rank = (2 + 2 * step) * per + h
             ready([rank], (0, 1))
             project([rank], xg, ((wv, pv), (wg, ps)), False)
             twin, index = rank + per, block(other + 1 - 2 * core, h)
             arrived(xg.at[index], recv_x.at[index])
+            line_send(xg.at[index, part_rows(part)], other + 1 - 2 * core, core == h)
             ready([twin], (0, 1))
             project([twin], xg, ((wv, pv), (wg, ps)), False)
-
-    for other in planes:
-        sends.start(xg.at[other * 2 + core], lg_out.at[outer, core], recv_l.at[outer, core], level(other))
 
     def gate(i, carry):
         c, r = lax.div(i, tokens // ROWS), lax.rem(i, tokens // ROWS)
@@ -327,6 +338,16 @@
     send_sums(stat2, recv_s2)
     outs = [pltpu.make_async_copy(act, act_out, out_sems.at[0])]
     outs[0].start()
+
+    def line_here(source, h, piece):
+        ref = lg_out.at[source, h, part_rows(piece)]
+        arrived(ref, recv_l.at[source, h, piece])
+        return ref
+
+    for source in planes:
+        ref = line_here(source, core, part)
+        for other in across + [sibling]:
+            sends.start(ref, ref, recv_l.at[source, core, part], home(other))
     first_mean, second_mean = take_sums(stat2, recv_s2)
     sum_a[...] = to_rows(first_mean)
     sum_b[...] = to_rows(second_mean)
@@ -371,12 +392,11 @@
     outs.append(pltpu.make_async_copy(gt, gt_out, out_sems.at[2]))
     outs.append(pltpu.make_async_copy(xg, xg_out, out_sems.at[3]))
     outs.append(pltpu.make_async_copy(gg, gg_out, out_sems.at[4]))
+    outs.append(pltpu.make_async_copy(hp, hp_out, out_sems.at[8]))
+    outs.append(pltpu.make_async_copy(gc, gc_out, out_sems.at[9]))
     for copy in outs[1:]:
         copy.start()
 
-    for other in planes:
-        arrived(lg_out.at[other, core], recv_l.at[other, core])
-        sends.start(lg_out.at[other, core], lg_out.at[other, core], recv_l.at[other, core], home(sibling))
     own_lefts = [pltpu.make_async_copy(xg.at[outer * 2 + h], lg_out.at[outer, h], out_sems.at[6 + h]) for h in range(2)]
     for copy in own_lefts:
         copy.start()
@@ -388,26 +408,20 @@
             arrived(crossed.at[b], recv.at[b])
             sends.start(crossed.at[b], crossed.at[b], recv.at[b], home(sibling))
 
-    def tap_sums(c, carry):
-        def step(r, sums):
-            row = pl.multiple_of(r * 8, 8)
-            grad = gc[c, pl.ds(pl.multiple_of(row + PAD, 8), 8), :]
-            return tuple(sums[k] + hp[c, pl.ds(row + (PAD + k - radius), 8), :] * grad for k in range(conv))
-
-        sums = lax.fori_loop(0, tokens // 8, step, tuple(jnp.zeros((8, LANES), F32) for _ in range(conv)))
-        for k in range(conv):
-            small[c, k : k + 1, :] = jnp.sum(sums[k], axis=0, keepdims=True)
-        return carry
-
-    lax.fori_loop(0, n_lane, tap_sums, 0)
     outs.append(pltpu.make_async_copy(small, small_out, out_sems.at[5]))
     outs[-1].start()
     for crossed, recv in ((px_out, recv_px), (pg_out, recv_pg)):
         for b in mine:
             twin = b + 1 - 2 * core
             arrived(crossed.at[twin], recv.at[twin])
-    for other in planes:
-        arrived(lg_out.at[other, 1 - core], recv_l.at[other, 1 - core])
+    for source in planes:
+        for step in range(1, n_y):
+            piece = lax.rem(part + step, n_y)
+            ref = line_here(source, core, piece)
+            sends.start(ref, ref, recv_l.at[source, core, piece], home(sibling))
+    for source in planes:
+        for piece in range(n_y):
+            line_here(source, 1 - core, piece)
     sends.drain()
     for copy in outs:
         copy.wait()
@@ -422,7 +436,7 @@
     per, n_lane, n_y = n_seq // n_tp, channels // LANES, n_tp // 2
     tap_cells = jnp.pad(taps.astype(F32), ((0, 1), (0, 0))).reshape(conv + 1, n_lane, LANES).transpose(1, 0, 2)
     gain_cells = ln_gain.reshape(n_lane, 1, LANES)
-    n_sends = 2 * (per * n_y + 1 + (n_y - 1) * per * 2 + n_y) + 4 + 2 * (n_tp - 1) + 2 * (n_outer - 1)
+    n_sends = 2 * (per * n_y + 1 + (n_y - 1) * per * 2 + n_y) + 4 + 2 * (n_tp - 1) + 2 + 2 * (n_y - 1) * per + (n_outer - 1) * (2 * n_y - 1)
     any_spec, vmem_spec = pl.BlockSpec(memory_space=pl.ANY), pl.BlockSpec(memory_space=pltpu.VMEM)
     lanes = lambda rows, dtype=F32: pltpu.VMEM((n_lane, rows, LANES), dtype)
     dma = lambda *shape: pltpu.SemaphoreType.DMA(shape)
@@ -431,6 +445,7 @@
         ((n_tp, tokens, width), BF16), ((n_tp, tokens, width), BF16), ((n_outer, 2, tokens, width), BF16),
         ((tokens, channels), BF16), ((tokens, channels), BF16), ((tokens, channels), BF16),
         ((n_lane, conv + 1, LANES), F32),
+        ((n_lane, tokens + 2 * PAD, LANES), F32), ((n_lane, tokens + 2 * PAD, LANES), F32),
     ]
     flops = 2 * 3 * tokens * own * n_tp * channels
     return pl.pallas_call(
@@ -448,8 +463,8 @@
             lanes(conv + 1),
             *[pltpu.VMEM((tokens, LANES), F32)] * 4,
             *[pltpu.VMEM((n_tp, 8, tokens), F32)] * 2,
-            dma(n_sends), dma(n_seq), dma(n_seq), dma(n_tp), dma(n_tp), dma(n_outer, 2), dma(2), dma(2), dma(n_tp), dma(n_tp),
-            dma(3, n_seq), dma(2, per), dma(8),
+            dma(n_sends), dma(n_seq), dma(n_seq), dma(n_tp), dma(n_tp), dma(n_outer, 2, n_y), dma(2), dma(2), dma(n_tp), dma(n_tp),
+            dma(3, n_seq), dma(2, per), dma(10),
         ],
         compiler_params=pltpu.CompilerParams(
             collective_id=0, has_side_effects=True, vmem_limit_bytes=63 * 1024 * 1024
@@ -479,10 +494,10 @@
 
 def back_kernel(
     n_outer, n_tp,
-    act_ref, gv_ref, gt_ref, xg_ref, gg_ref, px_ref, pg_ref, lg_ref, wv_ref, wg_ref, small_ref,
-    gi_out, gvw_out, ggw_out, gow_out, small_out,
+    act_ref, gv_ref, gt_ref, xg_ref, gg_ref, px_ref, pg_ref, lg_ref, wv_ref, wg_ref, small_ref, hp_ref, gc_ref,
+    gi_out, gvw_out, ggw_out, gow_out, taps_out, gain_out,
     own_left, pair_left, line_left, ag, rs, own_right, pair_right, gv, gt, weights, gi, gi_sent, gi_total,
-    racc, aacc, xacc, xs, xr, small, small_x, group, group_in, group_all, small_total,
+    racc, aacc, xacc, xs, xr, hp, gc, small, small_x, group, group_in, group_all, taps_total, gain_total,
     load_sems, left_sems, weight_sems, out_sems,
     ag_send, ag_recv, rs_send, rs_recv, xr_send, xr_recv, swap_send, swap_recv, gi_send, gi_recv,
     sx_send, sx_recv, s1_send, s1_recv, s2_send, s2_recv,
@@ -540,7 +555,7 @@
         load(act_ref.at[:, lead], own_right.at[0], load_sems.at[5]),
         load(act_ref.at[:, trail], own_right.at[1], load_sems.at[6]),
         load(gv_ref.at[:, lead], own_right.at[2], load_sems.at[7]),
-        load(small_ref, small, load_sems.at[8]),
+        load(small_ref, small, load_sems.at[8]), load(hp_ref, hp, load_sems.at[9]), load(gc_ref, gc, load_sems.at[10]),
     ]
     lefts = []
     for d in range(n):
@@ -570,8 +585,7 @@
         remote(src, pair_right.at[j], swap_send.at[j], swap_recv.at[j], facing)
         for j, src in enumerate((act_ref.at[:, lead], act_ref.at[:, trail], gv_ref.at[:, lead]))
     ]
-    small_swap = remote(small_ref, small_x, sx_send.at[0], sx_recv.at[0], facing)
-    small_swap.start()
+    small_swap = remote(small, small_x, sx_send.at[0], sx_recv.at[0], facing)
     for copy in swaps:
         copy.start()
 
@@ -605,18 +619,22 @@
 
     for copy in rights:
         copy.wait()
-    small_swap.wait_recv()
-    rows = group.shape[2]
-    for g in range(n):
-        group[g] = small[:, g * rows : (g + 1) * rows, :] + small_x[:, g * rows : (g + 1) * rows, :]
-    group_in[z] = group[z]
-    for step in range(1, n):
-        other = lax.rem(z + step, n)
-        remote(group.at[other], group_in.at[z], s1_send.at[step], s1_recv.at[z], level(other)).start()
+    n_lane, rows, conv = small.shape[0], group.shape[2], small.shape[1] - 1
+    radius = conv // 2
+
+    def tap_sums(c):
+        def step(r, sums):
+            row = pl.multiple_of(r * 8, 8)
+            grad = gc[c, pl.ds(pl.multiple_of(row + PAD, 8), 8), :]
+            return tuple(sums[k] + hp[c, pl.ds(row + (PAD + k - radius), 8), :] * grad for k in range(conv))
+
+        zeros = tuple(jnp.zeros((8, LANES), F32) for _ in range(conv))
+        sums = lax.fori_loop(0, (hp.shape[1] - 2 * PAD) // 8, step, zeros)
+        for k in range(conv):
+            small[c, k : k + 1, :] = jnp.sum(sums[k], axis=0, keepdims=True)
+
     for copy in lefts:
         copy.wait()
-    for copy in swaps:
-        copy.wait_recv()
 
     def partial_rows(j, d):
         tensor = lax.div(j, 2)
@@ -678,6 +696,8 @@
                 arrived(ag.at[j, z + k], ag_recv.at[j, z + k])
                 pl.when(z > 0)(lambda: ag_left(k, j).start())
 
+            pl.when(index == 0)(lambda: arrived(pair_right.at[j], swap_recv.at[j]))
+
             @pl.when(jnp.logical_and(z < last, k > z))
             def _():
                 reduce_step(j, n + z - k, z > 0, rs_right)
@@ -693,6 +713,22 @@
         loop(JOBS, job)
 
         @pl.when(index == 0)
+        def _():
+            loop(n_lane, tap_sums)
+            loop(JOBS, own_rows)
+            small_swap.start()
+
+        @pl.when(index == 1)
+        def _():
+            small_swap.wait_recv()
+            for g in range(n):
+                group[g] = small[:, g * rows : (g + 1) * rows, :] + small_x[:, g * rows : (g + 1) * rows, :]
+            group_in[z] = group[z]
+            for step in range(1, n):
+                other = lax.rem(z + step, n)
+                remote(group.at[other], group_in.at[z], s1_send.at[step], s1_recv.at[z], level(other)).start()
+
+        @pl.when(index == 2)
         def _():
             for step in range(1, n):
                 other = lax.rem(z + step, n)
@@ -703,7 +739,6 @@
             group_all[z] = total
             for step in range(1, n):
                 remote(group_all.at[z], group_all.at[z], s2_send.at[step], s2_recv.at[z], level(lax.rem(z + step, n))).start()
-            loop(JOBS, own_rows)
 
     loop(last, period)
 
@@ -721,15 +756,20 @@
         other = lax.rem(z + step, n)
         arrived(group_all.at[other], s2_recv.at[other])
     for g in range(n):
-        for c in range(small.shape[0]):
-            small_total[g * rows : (g + 1) * rows, c * LANES : (c + 1) * LANES] = group_all[g, c]
-    outs.append(load(small_total, small_out, out_sems.at[1]))
+        kept = min(rows, conv - g * rows)
+        for c in range(n_lane):
+            columns = slice(c * LANES, (c + 1) * LANES)
+            taps_total[g * rows : g * rows + kept, columns] = group_all[g, c, :kept]
+            if kept < rows:
+                gain_total[:, columns] = group_all[g, c, kept:]
+    outs.append(load(taps_total, taps_out, out_sems.at[1]))
+    outs.append(load(gain_total, gain_out, out_sems.at[8]))
 
     results = ((gvw_out, trail), (ggw_out, lead), (ggw_out, trail))
     for j, (ref, columns) in enumerate(results):
         arrived(xr.at[j], xr_recv.at[j])
-        aacc[j] += xr[j].astype(F32)
-        outs.append(load(aacc.at[j], ref.at[:, columns], out_sems.at[2 + j]))
+        xr[j] = (aacc[j] + xr[j].astype(F32)).astype(BF16)
+        outs.append(load(xr.at[j], ref.at[:, columns], out_sems.at[2 + j]))
     results = ((gow_out, lead), (gow_out, trail), (gvw_out, lead))
     for j, (ref, columns) in enumerate(results):
         @pl.when(z > 0)
@@ -742,7 +782,8 @@
             arrived(rs.at[j, n], rs_recv.at[j, n])
             racc[j] += rs[j, n].astype(F32)
 
-        outs.append(load(racc.at[j], ref.at[:, columns], out_sems.at[5 + j]))
+        rs[j, z] = racc[j].astype(BF16)
+        outs.append(load(rs.at[j, z], ref.at[:, columns], out_sems.at[5 + j]))
 
     def sent(j):
         def step(k):
@@ -765,7 +806,7 @@
         copy.wait()
 
 
-def back(act, gv, gt, xg, gg, px, pg, lg, w_value, w_gate, small):
+def back(act, gv, gt, xg, gg, px, pg, lg, w_value, w_gate, small, hp, gc):
     n, n_tp = lax.axis_size("outer"), lax.axis_size("tp")
     n_seq, tokens, width = xg.shape
     channels = act.shape[1]
@@ -774,13 +815,13 @@
     any_spec = pl.BlockSpec(memory_space=pl.ANY)
     dma = lambda *shape: pltpu.SemaphoreType.DMA(shape)
     bf, wide = (lambda *shape: pltpu.VMEM(shape, BF16)), (lambda *shape: pltpu.VMEM(shape, F32))
-    out_shapes = [((tokens, width * per), BF16)] + [((width, channels), F32)] * 3 + [((n_small, channels), F32)]
+    out_shapes = [((tokens, width * per), BF16)] + [((width, channels), BF16)] * 3 + [((n_small - 1, channels), F32), ((1, channels), F32)]
     flops = 2 * 5 * tokens * width * n_seq * channels
     return pl.pallas_call(
         functools.partial(back_kernel, n, n_tp),
         name="back",
         out_shape=[jax.ShapeDtypeStruct(shape, dtype) for shape, dtype in out_shapes],
-        in_specs=[any_spec] * 11,
+        in_specs=[any_spec] * 13,
         out_specs=[any_spec] * len(out_shapes),
         scratch_shapes=[
             bf(2, n, tokens, width), bf(2, n, tokens, width), bf(n, 2, tokens, width),
@@ -789,9 +830,10 @@
             bf(n_tp, per, tokens, width), bf((n_tp - 1) * per, tokens, width), bf(tokens, width * per),
             wide(JOBS, width, half), wide(JOBS, width, half), wide(JOBS, width, half),
             bf(JOBS, width, half), bf(JOBS, width, half),
+            wide(*hp.shape), wide(*gc.shape),
             wide(n_lane, n_small, LANES), wide(n_lane, n_small, LANES),
-            *[wide(n, n_lane, rows, LANES)] * 3, wide(n_small, channels),
-            dma(9), dma(5, n), dma(2, 2), dma(8),
+            *[wide(n, n_lane, rows, LANES)] * 3, wide(n_small - 1, channels), wide(1, channels),
+            dma(11), dma(5, n), dma(2, 2), dma(9),
             dma(2, JOBS, n), dma(JOBS, n), dma(JOBS, n + 1), dma(JOBS, n + 1), dma(JOBS), dma(JOBS), dma(JOBS), dma(JOBS),
             dma((n_tp - 1) * per), dma(n_tp, per),
             dma(1), dma(1), dma(n), dma(n), dma(n), dma(n),
@@ -800,15 +842,16 @@
             collective_id=1, has_side_effects=True, vmem_limit_bytes=63 * 1024 * 1024
         ),
         cost_estimate=pl.CostEstimate(flops=flops, bytes_accessed=60 * 2**20, transcendentals=0),
-    )(act, gv, gt, xg, gg, px, pg, lg, w_value, w_gate, small)
+    )(act, gv, gt, xg, gg, px, pg, lg, w_value, w_gate, small, hp, gc)
 
 
 def local(inputs, w_value, w_gate, taps, ln_gain, w_out, grad_out):
-    xg, gg, px, pg, lg, act, gv, gt, small = front(inputs, w_value, w_gate, taps, ln_gain, w_out, grad_out)
-    grad_input, grad_value_w, grad_gate_w, grad_out_w, token_sums = back(
-        act, gv, gt, xg, gg, px, pg, lg, w_value, w_gate, small
+    xg, gg, px, pg, lg, act, gv, gt, small, hp, gc = front(inputs, w_value, w_gate, taps, ln_gain, w_out, grad_out)
+    grad_input, grad_value_w, grad_gate_w, grad_out_w, grad_taps, grad_gain = back(
+        act, gv, gt, xg, gg, px, pg, lg, w_value, w_gate, small, hp, gc
     )
-    return (grad_input, grad_value_w, grad_gate_w, grad_out_w, token_sums[:-1], token_sums[-1])
+    weights = [value.astype(F32) for value in (grad_value_w, grad_gate_w, grad_out_w)]
+    return (grad_input, *weights, grad_taps, grad_gain[0])
 
 
 def solution(mesh):

time: 282 us -> 241 us (0.85)
  Pallas kernels: 264 us -> 226 us
  local copies, waits for them, and re-layouts: 10.4 us -> 2.24 us
  other arithmetic: 1.5 us -> 7.51 us
    pallas_call x1, Pallas kernels: 115 us -> 78.3 us  [front(): pl.pallas_call(functools.partial(front_kernel, n_outer, n_tp, conv), name...]
    unnamed x13, local copies, waits for them, and re-layouts: 8.94 us -> 2.24 us
    convert_element_type x0 -> x3, other arithmetic: none -> 6.01 us  [local(): value.astype(F32)]
where the time goes in v3:
time: 241 us; the launch traced here: 236 us
  Pallas kernels  226 us (94%)
  other arithmetic  7.51 us (3%)
    pallas_call x1, Pallas kernels, back(): pl.pallas_call(functools.partial(back_kernel, n, n_tp), name='back', out_...  148 us
    pallas_call x1, Pallas kernels, front(): pl.pallas_call(functools.partial(front_kernel, n_outer, n_tp, conv), name...  78.3 us
    convert_element_type x3, other arithmetic, local(): value.astype(F32)  6.01 us

profile of v3, /device:TPU:19, one launch (start us, length us, event | category | flops | bytes accessed | tf_op | source)
XLA Modules:
  0.0 236.4 jit_solution(15176627165414300615)
XLA Ops:
  0.6 1.5 bitcast_bitcast_fusion.taps_ref
  2.1 78.3 %front.1 = (bf16[8,512,512]{2,1,0:T(8,128)(2,1)}, bf16[8,512,512]{2,1,0:T(8,128)(2,1)}, bf16[4,512,512]{2,1,0:T(8,128)(2,1)}, bf16[4,512,512]{2,1,0:T(8,128)(2,1...) custom-call(bf16[512,1024]{1,0:T(8,128)(2,1)} %x_ref.1, ...), custom_call_target="tpu_custom_call" | custom-call | flops 12884901888 | bytes 41943040 | tf_op jit(solution)/shard_map/front/pallas_call | solution.py:451
  80.5 147.7 %back.1 = (bf16[512,1024]{1,0:T(8,128)(2,1)}, bf16[512,1024]{1,0:T(8,128)(2,1)}, bf16[512,1024]{1,0:T(8,128)(2,1)}, bf16[512,1024]{1,0:T(8,128)(2,1)}, f32[31,1024]{1,0:T(8,128)}, /*index=5*/f32[1,1024]{1,0:T(1,128)}) custom-call(bf16[512,1024]{1,0:T(8,128)(2,1)} %get-tuple-element.23.act_ref, bf16[512,1024]{1,0:T(8,128)(2,1)} %get-tuple-element.24.gv_ref, ...), custom_call_target="tpu_custom_call" | custom-call | flops 21474836480 | bytes 62914560 | tf_op jit(solution)/shard_map/back/pallas_call | solution.py:820
  228.2 0.0 copy-start.1
  228.2 2.9 %convert_element_type.12 = f32[512,1024]{1,0:T(8,128)} convert(bf16[512,1024]{1,0:T(8,128)(2,1)} %get-tuple-element.35) | non-fusion elementwise | flops 524288 | bytes 3145728 | tf_op jit(solution)/shard_map/convert_element_type | solution.py:853
  231.1 0.0 copy-done.1
  231.1 0.0 copy-start
  231.1 1.6 convert_element_type.13
  232.6 0.0 copy-done
  232.6 0.0 copy-start.2
  232.6 0.0 copy-start.3
  232.7 0.0 copy-start.4
  232.7 1.6 convert_element_type.14
  234.2 0.0 copy-done.2
  234.2 1.0 copy.19
  235.2 0.0 copy-done.3
  235.2 0.7 copy.20
  235.9 0.0 copy-done.4
  235.9 0.6 copy.21
Async XLA Ops:
  228.2 2.9 %copy-start.1 = (bf16[512,1024]{1,0:T(8,128)(2,1)S(1)}, bf16[512,1024]{1,0:T(8,128)(2,1)}, u32[]{:S(2)}) copy-start(bf16[512,1024]{1,0:T(8,128)(2,1)} %get-tuple-element.36) | copy-start | bytes 3145732
  231.1 1.6 copy-start
  232.6 1.6 copy-start.2
  232.6 2.5 %copy-start.3 = (f32[31,1024]{1,0:T(8,128)S(1)}, f32[31,1024]{1,0:T(8,128)}, u32[]{:S(2)}) copy-start(f32[31,1024]{1,0:T(8,128)} %get-tuple-element.50) | copy-start | bytes 380932
  232.7 3.2 %copy-start.4 = (f32[1,1024]{1,0:T(1,128)S(1)}, f32[1,1024]{1,0:T(1,128)}, u32[]{:S(2)}) copy-start(f32[1,1024]{1,0:T(1,128)} %get-tuple-element.39) | copy-start | bytes 12292

commit v4 on v1

v4 whole, which is shorter than its diff:
```python
import functools

import jax
import jax.numpy as jnp
from jax import lax
from jax.experimental import pallas as pl
from jax.experimental.pallas import tpu as pltpu
from jax.sharding import Mesh, PartitionSpec as P

MESH = pl.DeviceIdType.MESH
SP = ("outer", "pair")
AXES = ("outer", "pair", "tp")
LANES = 128
PAD = 16
ROWS = 64
F32, BF16 = jnp.float32, jnp.bfloat16


def sigmoid(value):
    return 1.0 / (1.0 + jnp.exp(-value))


def dot(left, right):
    return jnp.dot(left, right, preferred_element_type=F32)


class Sends:
    def __init__(self, sems):
        self.sems, self.open = sems, []

    def start(self, src, dst, recv, device):
        copy = pltpu.make_async_remote_copy(
            src_ref=src, dst_ref=dst, send_sem=self.sems.at[len(self.open)],
            recv_sem=recv, device_id=device, device_id_type=MESH,
        )
        copy.start()
        self.open.append((copy, None))

    def start_if(self, cond, src, dst, recv, device):
        copy = pltpu.make_async_remote_copy(
            src_ref=src, dst_ref=dst, send_sem=self.sems.at[len(self.open)],
            recv_sem=recv, device_id=device, device_id_type=MESH,
        )
        pl.when(cond)(copy.start)
        self.open.append((copy, cond))

    def drain(self):
        for copy, cond in self.open:
            if cond is None:
                copy.wait_send()
            else:
                pl.when(cond)(copy.wait_send)


def arrived(ref, recv):
    pltpu.make_async_copy(ref, ref, recv).wait()


JOBS = 3


def dot_tokens(left, right):
    return lax.dot_general(left, right, (((0,), (0,)), ((), ())), preferred_element_type=F32)


def dot_channels(left, right):
    return lax.dot_general(left, right, (((1,), (1,)), ((), ())), preferred_element_type=F32)


def loop(count, body):
    def step(index, carry):
        body(index)
        return carry

    lax.fori_loop(0, count, step, 0)


def kernel(
    n, n_tp, conv,
    x_ref, g_ref, wv_ref, wg_ref, wo_ref, taps_in, gain_ref,
    gi_out, gvw_out, ggw_out, gow_out, taps_out, gain_out, px_in, line_in, gi_in,
    taps_ref, both, weights, pool, hp, gc, ag, rs, own_right, pair_right, pair_left, line, gi_sent, gi_own, gi_total, xs, xr,
    sum_a, sum_b, mean_b, inv_b, stat1, stat2, small, small_x, group, group_in, group_all, taps_total, gain_total,
    send_sems, recv_x, recv_g, recv_px, recv_line, recv_h, recv_c, recv_s1, recv_s2, own_sems, weight_sems,
    left_sems, line_sems, out_sems,
    ag_send, ag_recv, rs_send, rs_recv, xr_send, xr_recv, swap_send, swap_recv, gi_send, gi_recv,
    sx_send, sx_recv, s1_send, s1_recv, s2_send, s2_recv,
):
    z, pair, tp = (lax.axis_index(name) for name in AXES)
    last, mirror = n - 1, n - 1 - z
    seq, n_seq, per = z * 2 + pair, n * 2, (n * 2) // n_tp
    tokens, width, half = both.shape[2], both.shape[3], own_right.shape[2]
    n_lane, total = hp.shape[0], width * n_seq
    n_half = n_lane // 2
    sibling, core, n_y = tp + 1 - 2 * lax.rem(tp, 2), lax.rem(tp, 2), n_tp // 2
    across = [lax.rem(tp + 2 * step, n_tp) for step in range(1, n_y)]
    radius = conv // 2
    before, after = seq - 1, seq + 1
    has_before, has_after = seq > 0, seq < n_seq - 1
    home = lambda index: (z, pair, index)
    beside = lambda index: (lax.div(index, 2), lax.rem(index, 2), tp)
    level = lambda index: (index, pair, tp)
    facing = (z, 1 - pair, tp)
    planes = [lax.rem(z + step, n) for step in range(1, n)]
    gg, xg = both.at[0], both.at[1]
    PV, PS, GA, CV = 0, n_lane, 2 * n_lane, 3 * n_lane

    barrier = pltpu.get_barrier_semaphore()

    def greet(device):
        pl.semaphore_signal(barrier, inc=1, device_id=device, device_id_type=MESH)

    for step in range(1, n_tp):
        greet(home(lax.rem(tp + step, n_tp)))
    pl.when(has_before)(lambda: greet(beside(before)))
    pl.when(has_after)(lambda: greet(beside(after)))
    greet(facing)
    for other in planes:
        greet(level(other))

    def load(src, dst, sem):
        copy = pltpu.make_async_copy(src, dst, sem)
        copy.start()
        return copy

    def remote(src, dst, send, recv, device):
        return pltpu.make_async_remote_copy(
            src_ref=src, dst_ref=dst, send_sem=send, recv_sem=recv, device_id=device, device_id_type=MESH
        )

    block = lambda b, h: b * per + h
    order = [tp, sibling]
    for other in across:
        order += [other, other + 1 - 2 * core]

    places = [(False, r) for r in range(2 * per)] + [(True, r) for r in range(2 * per)]
    for wanted in (False, True):
        for step in range(n_y - 1):
            for h in range(per):
                places += [(wanted, (2 + 2 * step) * per + h), (wanted, (3 + 2 * step) * per + h)]

    def streams(turn):
        wanted, rank = places[turn]
        index = block(order[rank // per], rank % per)
        row = pl.multiple_of(index * width, width)
        return index, [
            pltpu.make_async_copy(ref.at[pl.ds(row, width), :], weights.at[turn % 2, i], weight_sems.at[turn % 2, i])
            for i, ref in enumerate((wo_ref,) if wanted else (wv_ref, wg_ref))
        ]

    for c in range(n_lane):
        taps_ref[c, 0:conv, :] = taps_in[:, c * LANES : (c + 1) * LANES].astype(F32)

    def gain_of(c):
        return gain_ref[:, pl.ds(pl.multiple_of(c * LANES, LANES), LANES)]

    owns = []
    for name, (hbm, vmem) in enumerate(((x_ref, xg), (g_ref, gg))):
        owns.append([
            load(hbm.at[:, pl.ds(h * width, width)], vmem.at[block(tp, h)], own_sems.at[name, h]) for h in range(per)
        ])
    for copy in streams(0)[1]:
        copy.start()

    count = n_tp - 1 + 1 + n - 1 + has_before.astype(jnp.int32) + has_after.astype(jnp.int32)
    pl.semaphore_wait(barrier, count)

    sends = Sends(send_sems)
    for hbm, vmem, recv in ((x_ref, xg, recv_x), (g_ref, gg, recv_g)):
        for h in range(per):
            src, index = hbm.at[:, pl.ds(h * width, width)], block(tp, h)
            for other in [sibling] + across:
                sends.start(src, vmem.at[index], recv.at[index], home(other))
    crossing = pl.multiple_of((1 - pair) * width, width)
    sends.start(x_ref.at[:, pl.ds(crossing, width)], px_in.at[tp], recv_px.at[tp], facing)

    part, n_part = lax.div(tp, 2), tokens // n_y

    def part_rows(index):
        start = index * n_part
        return pl.ds(start if isinstance(index, int) else pl.multiple_of(start, n_part), n_part)


    def line_send(tensor, src, b, cond):
        sends.start_if(
            jnp.logical_and(cond, b != z), src, line_in.at[tensor, z, core, part_rows(part)],
            recv_line.at[tensor, z, core, part], level(b),
        )

    column = pl.multiple_of(core * width, width)
    line_send(1, x_ref.at[part_rows(part), pl.ds(column, width)], tp, True)

    turns = iter(range(len(places)))

    def project(left):
        turn = next(turns)
        wanted, rank = places[turn]
        index, copies = streams(turn)
        if turn + 1 < len(places):
            for copy in streams(turn + 1)[1]:
                copy.start()
        for copy in copies:
            copy.wait()

        def body(j):
            cols = pl.ds(pl.multiple_of(j * 256, 256), 256)
            for i, base in enumerate((GA,) if wanted else (PV, PS)):
                value = dot(left[index], weights[turn % 2, i, :, cols])
                for side in range(2):
                    piece = value[:, side * LANES : (side + 1) * LANES]
                    if rank == 0:
                        pool[base + 2 * j + side] = piece
                    else:
                        pool[base + 2 * j + side] += piece

        loop(n_lane // 2, body)

    def land(vmem, recv, b, h):
        index = block(b, h)
        arrived(vmem.at[index], recv.at[index])
        sends.start(vmem.at[index], vmem.at[index], recv.at[index], home(sibling))

    def near(tensor, vmem, recv):
        for copy in owns[1 - tensor]:
            copy.wait()
        for h in range(per):
            project(vmem)
        for h in range(per):
            index = block(sibling, h)
            arrived(vmem.at[index], recv.at[index])
        if tensor == 1:
            line_send(1, xg.at[block(sibling, core), part_rows(part)], sibling, True)
        for h in range(per):
            project(vmem)

    def far(tensor, vmem, recv, between):
        for other in across:
            for h in range(per):
                if other is across[-1] and h == per - 1:
                    between()
                land(vmem, recv, other, h)
                line_send(tensor, vmem.at[block(other, h), part_rows(part)], other, core == h)
                if tensor == 1:
                    sends.start_if(h != pair, vmem.at[block(other, h)], px_in.at[other], recv_px.at[other], facing)
                project(vmem)
                index = block(other + 1 - 2 * core, h)
                arrived(vmem.at[index], recv.at[index])
                line_send(tensor, vmem.at[index, part_rows(part)], other + 1 - 2 * core, core == h)
                project(vmem)

    near(1, xg, recv_x)
    near(0, gg, recv_g)
    far(1, xg, recv_x, lambda: None)

    def gate(i):
        c, r = lax.div(i, tokens // ROWS), lax.rem(i, tokens // ROWS)
        rows = pl.ds(pl.multiple_of(r * ROWS, ROWS), ROWS)
        sig = sigmoid(pool[PS + c, rows, :])
        pool[PS + c, rows, :] = sig
        hp[c, pl.ds(pl.multiple_of(r * ROWS + PAD, 8), ROWS), :] = (pool[PV + c, rows, :] * sig).astype(BF16).astype(F32)

    loop(n_lane * (tokens // ROWS), gate)

    def halo(buffer, recv):
        @pl.when(jnp.logical_not(has_before))
        def _():
            buffer[:, 0:PAD, :] = jnp.zeros((n_lane, PAD, LANES), F32)

        @pl.when(jnp.logical_not(has_after))
        def _():
            buffer[:, PAD + tokens : 2 * PAD + tokens, :] = jnp.zeros((n_lane, PAD, LANES), F32)

        sends.start_if(has_after, buffer.at[:, pl.ds(tokens, PAD), :], buffer.at[:, pl.ds(0, PAD), :], recv.at[0], beside(after))
        sends.start_if(has_before, buffer.at[:, pl.ds(PAD, PAD), :], buffer.at[:, pl.ds(PAD + tokens, PAD), :], recv.at[1], beside(before))

    def halo_here(buffer, recv):
        pl.when(has_before)(lambda: arrived(buffer.at[:, pl.ds(0, PAD), :], recv.at[0]))
        pl.when(has_after)(lambda: arrived(buffer.at[:, pl.ds(PAD + tokens, PAD), :], recv.at[1]))

    halo(hp, recv_h)
    line_send(0, g_ref.at[part_rows(part), pl.ds(column, width)], tp, True)
    line_send(0, gg.at[block(sibling, core), part_rows(part)], sibling, True)

    def convolve(r):
        rows = pl.ds(pl.multiple_of(r * ROWS, ROWS), ROWS)

        def lane(c, carry):
            first, second = carry
            value = jnp.zeros((ROWS, LANES), F32)
            for k in range(conv):
                value = value + taps_ref[c, k : k + 1, :] * hp[c, pl.ds(r * ROWS + (PAD + k - radius), ROWS), :]
            pool[CV + c, rows, :] = value
            return first + value, second + value * value

        zero = jnp.zeros((ROWS, LANES), F32)
        first, second = lax.fori_loop(0, n_lane, lane, (zero, zero))
        sum_a[rows, :] = first
        sum_b[rows, :] = second

    def inner_rows(body):
        def step(r, carry):
            body(r)
            return carry

        lax.fori_loop(1, tokens // ROWS - 1, step, 0)

    inner_rows(convolve)
    halo_here(hp, recv_h)
    convolve(0)
    convolve(tokens // ROWS - 1)

    def to_row(value):
        return jnp.sum(value.T, axis=0, keepdims=True)

    def to_rows(row):
        return jnp.broadcast_to(row, (LANES, tokens)).T

    def send_sums(stat, recv):
        stat[tp, 0:1, :] = to_row(sum_a[...])
        stat[tp, 1:2, :] = to_row(sum_b[...])
        for step in range(1, n_tp):
            sends.start(stat.at[tp], stat.at[tp], recv.at[tp], home(lax.rem(tp + step, n_tp)))

    def take_sums(stat, recv):
        for step in range(1, n_tp):
            other = lax.rem(tp + step, n_tp)
            arrived(stat.at[other], recv.at[other])
        first, second = stat[0, 0:1, :], stat[0, 1:2, :]
        for other in range(1, n_tp):
            first, second = first + stat[other, 0:1, :], second + stat[other, 1:2, :]
        return first / total, second / total

    send_sums(stat1, recv_s1)

    lane_of = lambda c: pl.ds(pl.multiple_of(lax.rem(c, n_half) * LANES, LANES), LANES)

    def ag_right(k, j):
        return remote(ag.at[j, z - k], ag.at[j, z - k], ag_send.at[0, j, k], ag_recv.at[j, z - k], level(z + 1))

    def ag_left(k, j):
        return remote(ag.at[j, z + k], ag.at[j, z + k], ag_send.at[1, j, k], ag_recv.at[j, z + k], level(z - 1))

    def leave(j):
        pl.when(z < last)(lambda: ag_right(0, j).start())
        pl.when(z > 0)(lambda: ag_left(0, j).start())

    def activate():
        mean, square = take_sums(stat1, recv_s1)
        mean_b[...] = to_rows(mean)
        inv_b[...] = to_rows(lax.rsqrt(square - mean * mean + 1e-06))
        small[:, conv : conv + 1, :] = jnp.zeros((n_lane, 1, LANES), F32)

        def step(r):
            rows = pl.ds(pl.multiple_of(r * ROWS, ROWS), ROWS)
            mean_r, inv_r = mean_b[rows, :], inv_b[rows, :]

            def lane(c):
                normed = (pool[CV + c, rows, :] - mean_r) * inv_r
                pool[CV + c, rows, :] = normed
                scaled = normed * gain_of(c)
                ag[lax.div(c, n_half), z, rows, lane_of(c)] = (scaled * sigmoid(scaled)).astype(BF16)

            loop(n_lane, lane)

        loop(tokens // ROWS, step)

    far(0, gg, recv_g, activate)
    def backward(r, carry):
        rows = pl.ds(pl.multiple_of(r * ROWS, ROWS), ROWS)

        def lane(c, carry):
            first, second = carry
            normed = pool[CV + c, rows, :]
            gain = gain_of(c)
            scaled = normed * gain
            sig = sigmoid(scaled)
            grad_scaled = pool[GA + c, rows, :] * sig * (1.0 + scaled * (1.0 - sig))
            small[c, conv : conv + 1, :] += jnp.sum(grad_scaled * normed, axis=0, keepdims=True)
            grad_normed = grad_scaled * gain
            gc[c, pl.ds(pl.multiple_of(r * ROWS + PAD, 8), ROWS), :] = grad_normed
            return first + grad_normed, second + grad_normed * normed

        zero = jnp.zeros((ROWS, LANES), F32)
        first, second = lax.fori_loop(0, n_lane, lane, (zero, zero))
        sum_a[rows, :] = first
        sum_b[rows, :] = second
        return carry

    lax.fori_loop(0, tokens // ROWS, backward, 0)
    send_sums(stat2, recv_s2)

    def line_here(tensor, source, h, piece):
        ref = line_in.at[tensor, source, h, part_rows(piece)]
        arrived(ref, recv_line.at[tensor, source, h, piece])
        return ref

    def line_share(tensor):
        for source in planes:
            ref = line_here(tensor, source, core, part)
            for other in across + [sibling]:
                sends.start(ref, ref, recv_line.at[tensor, source, core, part], home(other))

    def line_pass(tensor):
        for source in planes:
            for step in range(1, n_y):
                piece = lax.rem(part + step, n_y)
                ref = line_here(tensor, source, core, piece)
                sends.start(ref, ref, recv_line.at[tensor, source, core, piece], home(sibling))

    def line_end(tensor):
        for source in planes:
            for piece in range(n_y):
                line_here(tensor, source, 1 - core, piece)

    line_share(1)
    mine = [tp] + across
    for b in mine:
        arrived(px_in.at[b], recv_px.at[b])
        sends.start(px_in.at[b], px_in.at[b], recv_px.at[b], home(sibling))
    first_mean, second_mean = take_sums(stat2, recv_s2)
    sum_a[...] = to_rows(first_mean)
    sum_b[...] = to_rows(second_mean)

    def finish(r):
        rows = pl.ds(pl.multiple_of(r * ROWS, ROWS), ROWS)
        padded = pl.ds(pl.multiple_of(r * ROWS + PAD, 8), ROWS)
        inv_r, first_r, second_r = inv_b[rows, :], sum_a[rows, :], sum_b[rows, :]

        def lane(c, carry):
            gc[c, padded, :] = inv_r * (gc[c, padded, :] - first_r - pool[CV + c, rows, :] * second_r)
            return carry

        lax.fori_loop(0, n_lane, lane, 0)

    finish(0)
    finish(tokens // ROWS - 1)
    halo(gc, recv_c)
    leave(0)
    leave(1)
    inner_rows(finish)

    def spread(r):
        rows = pl.ds(pl.multiple_of(r * ROWS, ROWS), ROWS)

        def lane(c, carry):
            value = jnp.zeros((ROWS, LANES), F32)
            for k in range(conv):
                value = value + taps_ref[c, k : k + 1, :] * gc[c, pl.ds(r * ROWS + (PAD + radius - k), ROWS), :]
            sig = pool[PS + c, rows, :]
            own_right[lax.div(c, n_half), rows, lane_of(c)] = (value * sig).astype(BF16)
            grad_gate = (value * pool[PV + c, rows, :] * sig * (1.0 - sig)).astype(BF16)

            @pl.when(c < n_half)
            def _():
                own_right[2, rows, lane_of(c)] = grad_gate

            @pl.when(c >= n_half)
            def _():
                ag[2, z, rows, lane_of(c)] = grad_gate

            return carry

        lax.fori_loop(0, n_lane, lane, 0)

    inner_rows(spread)
    halo_here(gc, recv_c)
    spread(0)
    spread(tokens // ROWS - 1)

    steps = n_tp * per

    def weight_copies(s, slot):
        b, h = lax.rem(tp + 1 + lax.div(s, per), n_tp), lax.rem(s, per)
        row = pl.multiple_of((b * per + h) * width, width)
        return [
            pltpu.make_async_copy(ref.at[pl.ds(row, width), :], weights.at[slot, i], weight_sems.at[slot, i])
            for i, ref in enumerate((wv_ref, wg_ref))
        ]

    for copy in weight_copies(0, 0):
        copy.start()
    for b in mine:
        twin = b + 1 - 2 * core
        arrived(px_in.at[twin], recv_px.at[twin])
    lefts = [load(px_in.at[d], pair_left.at[d], left_sems.at[d]) for d in range(n)]
    leave(2)
    swaps = [remote(own_right.at[j], pair_right.at[j], swap_send.at[j], swap_recv.at[j], facing) for j in range(JOBS)]
    for copy in swaps:
        copy.start()
    line_share(0)

    lead, trail = pl.ds(0, half), pl.ds(half, half)

    def input_step(s):
        slot = lax.rem(s, 2)

        @pl.when(s < steps - 1)
        def _():
            for copy in weight_copies(s + 1, 1 - slot):
                copy.start()

        for copy in weight_copies(s, slot):
            copy.wait()
        b, h = lax.rem(tp + 1 + lax.div(s, per), n_tp), lax.rem(s, per)
        value = dot_channels(own_right[0], weights[slot, 0, :, lead]) + dot_channels(own_right[1], weights[slot, 0, :, trail])
        value = value + dot_channels(own_right[2], weights[slot, 1, :, lead])
        value = (value + dot_channels(ag[2, z], weights[slot, 1, :, trail])).astype(BF16)

        @pl.when(s < steps - per)
        def _():
            gi_sent[s] = value
            remote(gi_sent.at[s], gi_in.at[tp, h], gi_send.at[s], gi_recv.at[tp, h], home(b)).start()

        @pl.when(s >= steps - per)
        def _():
            gi_own[h] = value

    loop(steps // 2, input_step)
    line_pass(1)
    for copy in lefts:
        copy.wait()
    rows = group.shape[2]

    def tap_sums(c):
        def step(r, sums):
            row = pl.multiple_of(r * 8, 8)
            grad = gc[c, pl.ds(pl.multiple_of(row + PAD, 8), 8), :]
            return tuple(sums[k] + hp[c, pl.ds(row + (PAD + k - radius), 8), :] * grad for k in range(conv))

        zeros = tuple(jnp.zeros((8, LANES), F32) for _ in range(conv))
        sums = lax.fori_loop(0, (hp.shape[1] - 2 * PAD) // 8, step, zeros)
        for k in range(conv):
            small[c, k : k + 1, :] = jnp.sum(sums[k], axis=0, keepdims=True)

    def keep(kind, j, value, add):
        for i in range(n_half):
            index, piece = (kind * JOBS + j) * n_half + i, value[:, i * LANES : (i + 1) * LANES]
            if add:
                pool[index, 0:width, :] += piece
            else:
                pool[index, 0:width, :] = piece

    def partial_rows(j, d):
        return dot_tokens(both[1, d * 2 + pair], own_right[j]) + dot_tokens(pair_left[d], pair_right[j])

    def own_rows(j):
        keep(0, j, partial_rows(j, z), False)
        tensor, cells = lax.div(j, 2), ag[j, z]
        keep(1, j, dot_tokens(both[tensor, z * 2 + pair], cells), False)
        keep(2, j, dot_tokens(both[tensor, z * 2 + 1 - pair], cells), False)

    def line_rows(j, source, side):
        tensor, cells = lax.div(j, 2), ag[j, source]
        keep(1, j, dot_tokens(line[side, tensor, pair], cells), True)
        keep(2, j, dot_tokens(line[side, tensor, 1 - pair], cells), True)

    def line_load(k, action):
        for side, (cond, source) in enumerate(((k <= z, z - k), (k <= mirror, z + k))):
            @pl.when(cond)
            def _():
                for tensor in range(2):
                    action(pltpu.make_async_copy(line_in.at[tensor, source], line.at[side, tensor], line_sems.at[side, tensor]))

    def rs_right(j, d):
        return remote(rs.at[j, d], rs.at[j, d], rs_send.at[j, d], rs_recv.at[j, d], level(z + 1))

    def rs_left(j, d):
        slot = jnp.where(d == z - 1, n, d)
        return remote(rs.at[j, d], rs.at[j, slot], rs_send.at[j, d], rs_recv.at[j, slot], level(z - 1))

    def reduce_step(j, d, waiting, copy):
        value = partial_rows(j, d)

        @pl.when(waiting)
        def _():
            arrived(rs.at[j, d], rs_recv.at[j, d])
            rs[j, d] = (value + rs[j, d].astype(F32)).astype(BF16)

        @pl.when(jnp.logical_not(waiting))
        def _():
            rs[j, d] = value.astype(BF16)

        copy(j, d).start()

    farthest = jnp.maximum(z, mirror)
    small_swap = remote(small, small_x, sx_send.at[0], sx_recv.at[0], facing)

    def add_lines(j, k):
        pl.when(k <= z)(lambda: line_rows(j, z - k, 0))
        pl.when(k <= mirror)(lambda: line_rows(j, z + k, 1))

        @pl.when(k == farthest)
        def _():
            for i in range(n_half):
                xs[j, :, i * LANES : (i + 1) * LANES] = pool[(2 * JOBS + j) * n_half + i, 0:width, :].astype(BF16)
            remote(xs.at[j], xr.at[j], xr_send.at[j], xr_recv.at[j], facing).start()

    def period(k, first):
        if not first:
            line_load(k, lambda copy: copy.start())

        def job(j):
            @pl.when(k <= z)
            def _():
                arrived(ag.at[j, z - k], ag_recv.at[j, z - k])
                pl.when(z < last)(lambda: ag_right(k, j).start())

            @pl.when(k <= mirror)
            def _():
                arrived(ag.at[j, z + k], ag_recv.at[j, z + k])
                pl.when(z > 0)(lambda: ag_left(k, j).start())

            if first:
                arrived(pair_right.at[j], swap_recv.at[j])

            @pl.when(jnp.logical_and(z < last, k > z))
            def _():
                reduce_step(j, n + z - k, z > 0, rs_right)

            @pl.when(jnp.logical_and(z > 0, k > mirror))
            def _():
                reduce_step(j, k - mirror - 1, z < last, rs_left)

            if not first:
                pl.when(j == 0)(lambda: line_load(k, lambda copy: copy.wait()))
                add_lines(j, k)

        loop(JOBS, job)

    period(1, True)
    loop(steps - steps // 2, lambda s: input_step(s + steps // 2))
    line_pass(0)
    loop(n_lane, tap_sums)
    line_end(1)
    line_end(0)
    line_load(1, lambda copy: copy.start())
    small_swap.start()
    loop(JOBS, own_rows)
    small_swap.wait_recv()
    for g in range(n):
        group[g] = small[:, g * rows : (g + 1) * rows, :] + small_x[:, g * rows : (g + 1) * rows, :]
    group_in[z] = group[z]
    for step in range(1, n):
        other = lax.rem(z + step, n)
        remote(group.at[other], group_in.at[z], s1_send.at[step], s1_recv.at[z], level(other)).start()
    line_load(1, lambda copy: copy.wait())
    loop(JOBS, lambda j: add_lines(j, 1))

    def share_sums():
        for step in range(1, n):
            other = lax.rem(z + step, n)
            arrived(group_in.at[other], s1_recv.at[other])
        value = group_in[0]
        for other in range(1, n):
            value = value + group_in[other]
        group_all[z] = value
        for step in range(1, n):
            remote(group_all.at[z], group_all.at[z], s2_send.at[step], s2_recv.at[z], level(lax.rem(z + step, n))).start()

    def later(index):
        pl.when(index == 1)(share_sums)
        period(index + 2, False)

    loop(last - 1, later)

    loop(steps - per, lambda s: remote(gi_sent.at[s], gi_in.at[tp, 0], gi_send.at[s], gi_recv.at[tp, 0], facing).wait_send())
    arrivals = []
    for step in range(1, n_tp):
        other = lax.rem(tp + step, n_tp)
        for h in range(per):
            arrived(gi_in.at[other, h], gi_recv.at[other, h])
            slot = (step - 1) * per + h
            arrivals.append(load(gi_in.at[other, h], gi_sent.at[slot], gi_send.at[slot]))
    for copy in arrivals:
        copy.wait()
    for h in range(per):
        value = gi_own[h].astype(F32)
        for step in range(1, n_tp):
            value = value + gi_sent[(step - 1) * per + h].astype(F32)
        gi_total[:, h * width : (h + 1) * width] = value.astype(BF16)
    outs = [load(gi_total, gi_out, out_sems.at[0])]
    for step in range(1, n):
        other = lax.rem(z + step, n)
        arrived(group_all.at[other], s2_recv.at[other])
    for g in range(n):
        kept = min(rows, conv - g * rows)
        for c in range(n_lane):
            columns = slice(c * LANES, (c + 1) * LANES)
            taps_total[g * rows : g * rows + kept, columns] = group_all[g, c, :kept]
            if kept < rows:
                gain_total[:, columns] = group_all[g, c, kept:]
    outs.append(load(taps_total, taps_out, out_sems.at[1]))
    outs.append(load(gain_total, gain_out, out_sems.at[8]))

    def settle(kind, j, slot, into):
        for i in range(n_half):
            cols = slice(i * LANES, (i + 1) * LANES)
            value = pool[(kind * JOBS + j) * n_half + i, 0:width, :]
            for ref in slot:
                value = value + ref[:, cols].astype(F32)
            into[:, cols] = value.astype(BF16)

    for j, (ref, columns) in enumerate(((gow_out, lead), (gow_out, trail), (ggw_out, trail))):
        arrived(xr.at[j], xr_recv.at[j])
        settle(1, j, (xr.at[j],), xr.at[j])
        outs.append(load(xr.at[j], ref.at[:, columns], out_sems.at[2 + j]))
    for j, (ref, columns) in enumerate(((gvw_out, lead), (gvw_out, trail), (ggw_out, lead))):
        lower, upper = rs.at[j, z], rs.at[j, n]
        pl.when(z > 0)(lambda: arrived(lower, rs_recv.at[j, z]))
        pl.when(z < last)(lambda: arrived(upper, rs_recv.at[j, n]))
        pl.when(z == 0)(lambda: settle(0, j, (upper,), lower))
        pl.when(z == last)(lambda: settle(0, j, (lower,), lower))
        pl.when(jnp.logical_and(z > 0, z < last))(lambda: settle(0, j, (lower, upper), lower))
        outs.append(load(lower, ref.at[:, columns], out_sems.at[5 + j]))

    def sent(j):
        def step(k):
            pl.when(jnp.logical_and(k <= z, z < last))(lambda: ag_right(k, j).wait_send())
            pl.when(jnp.logical_and(k <= mirror, z > 0))(lambda: ag_left(k, j).wait_send())
            pl.when(k > z)(lambda: rs_right(j, k).wait_send())
            pl.when(k < z)(lambda: rs_left(j, k).wait_send())

        loop(n, step)
        remote(xs.at[j], xr.at[j], xr_send.at[j], xr_recv.at[j], facing).wait_send()

    loop(JOBS, sent)
    for copy in swaps + [small_swap]:
        copy.wait_send()
    sends.drain()
    for step in range(1, n):
        remote(group.at[0], group_in.at[z], s1_send.at[step], s1_recv.at[z], facing).wait_send()
        remote(group_all.at[z], group_all.at[z], s2_send.at[step], s2_recv.at[z], facing).wait_send()
    for copy in outs:
        copy.wait()


def local(inputs, w_value, w_gate, taps, ln_gain, w_out, grad_out):
    n, n_tp = lax.axis_size("outer"), lax.axis_size("tp")
    n_seq = n * 2
    tokens, own = inputs.shape
    conv, channels = taps.shape
    width = own * n_tp // n_seq
    per, n_lane, n_y, half = n_seq // n_tp, channels // LANES, n_tp // 2, channels // 2
    n_sends = (
        2 * per * n_y + 1 + 2 + 2 + 2 * 3 * (n_y - 1) * per + (n_y - 1) * per + 4 + 2 * (n_tp - 1)
        + 2 * (n - 1) * (2 * n_y - 1) + n_y
    )
    any_spec, vmem_spec = pl.BlockSpec(memory_space=pl.ANY), pl.BlockSpec(memory_space=pltpu.VMEM)
    dma = lambda *shape: pltpu.SemaphoreType.DMA(shape)
    bf, wide = (lambda *shape: pltpu.VMEM(shape, BF16)), (lambda *shape: pltpu.VMEM(shape, F32))
    out_shapes = [
        ((tokens, own), BF16), *[((width, channels), BF16)] * 3, ((conv, channels), F32), ((1, channels), F32),
        ((n_tp, tokens, width), BF16), ((2, n, 2, tokens, width), BF16), ((n_tp, per, tokens, width), BF16),
    ]
    n_gi, rows = (n_tp - 1) * per, (conv + 1) // n
    results = pl.pallas_call(
        functools.partial(kernel, n, n_tp, conv),
        name="module_backward",
        out_shape=[jax.ShapeDtypeStruct(shape, dtype) for shape, dtype in out_shapes],
        in_specs=[any_spec] * 5 + [vmem_spec] * 2,
        out_specs=[any_spec] * len(out_shapes),
        scratch_shapes=[
            wide(n_lane, conv + 1, LANES), bf(2, n_seq, tokens, width), bf(2, 2, width, channels), wide(4 * n_lane + n_lane // 2, tokens, LANES),
            wide(n_lane, tokens + 2 * PAD, LANES), wide(n_lane, tokens + 2 * PAD, LANES),
            bf(JOBS, n, tokens, half), bf(JOBS, n + 1, width, half), bf(JOBS, tokens, half), bf(JOBS, tokens, half),
            bf(n, tokens, width), bf(2, 2, 2, tokens, width),
            bf(n_gi, tokens, width), bf(per, tokens, width), bf(tokens, own),
            bf(JOBS, width, half), bf(JOBS, width, half),
            *[wide(tokens, LANES)] * 4, *[wide(n_tp, 8, tokens)] * 2,
            wide(n_lane, conv + 1, LANES), wide(n_lane, conv + 1, LANES),
            *[wide(n, n_lane, rows, LANES)] * 3, wide(conv, channels), wide(1, channels),
            dma(n_sends), dma(n_seq), dma(n_seq), dma(n_tp), dma(2, n, 2, n_y), dma(2), dma(2), dma(n_tp), dma(n_tp),
            dma(2, per), dma(2, 2), dma(n), dma(2, 2), dma(9),
            dma(2, JOBS, n), dma(JOBS, n), dma(JOBS, n + 1), dma(JOBS, n + 1), dma(JOBS), dma(JOBS), dma(JOBS), dma(JOBS),
            dma(n_gi), dma(n_tp, per),
            dma(1), dma(1), dma(n), dma(n), dma(n), dma(n),
        ],
        compiler_params=pltpu.CompilerParams(
            collective_id=0, has_side_effects=True, vmem_limit_bytes=67043328
        ),
        cost_estimate=pl.CostEstimate(
            flops=2 * 8 * tokens * width * n_seq * channels, bytes_accessed=80 * 2**20, transcendentals=0
        ),
    )(inputs, grad_out, w_value, w_gate, w_out, taps, ln_gain.reshape(1, channels))
    parts = 4
    block = lambda shape: pl.BlockSpec((shape[0] // parts, shape[1]), lambda i: (i, 0))
    fixed = lambda shape: pl.BlockSpec(shape, lambda i: (0, 0))
    shapes = [shape for shape, dtype in out_shapes[:6]]
    specs = [block(shape) for shape in shapes[:4]] + [fixed(shape) for shape in shapes[4:]]

    def write(*refs):
        for source, target in zip(refs[:6], refs[6:]):
            target[...] = source[...].astype(target.dtype)

    written = pl.pallas_call(
        write,
        name="write_results",
        grid=(parts,),
        out_shape=[jax.ShapeDtypeStruct(shape, F32 if i else BF16) for i, shape in enumerate(shapes)],
        in_specs=specs,
        out_specs=specs,
        cost_estimate=pl.CostEstimate(flops=0, bytes_accessed=11 * 2**20, transcendentals=0),
    )(*results[:6])
    return (*written[:5], written[5][0])


def solution(mesh):
    count, across = mesh.devices.shape
    fine = Mesh(mesh.devices.reshape(count // 2, 2, across), AXES)
    in_specs = (P(SP, "tp"), P(None, "tp"), P(None, "tp"), P(None, "tp"), P("tp"), P(None, "tp"), P(SP, "tp"))
    out_specs = (P(SP, "tp"), P(SP, "tp"), P(SP, "tp"), P(SP, "tp"), P(None, "tp"), P("tp"))
    return jax.shard_map(local, mesh=fine, in_specs=in_specs, out_specs=out_specs, check_vma=False)
```

time: 375 us -> 221 us (0.59)
  waiting for transfers between devices: 198 us -> 0 us
  Pallas kernels: 79 us -> 220 us
  matrix products: 45.5 us -> 0 us
  local copies, waits for them, and re-layouts: 16.5 us -> 0 us
  other arithmetic: 13.6 us -> 0 us
  between operations: 13.9 us -> 0.75 us
  starting transfers between devices: 7.02 us -> 0 us
    pallas_call x1 -> x2, Pallas kernels: 79 us -> 220 us  [the longest x1 214 us: local(): pl.pallas_call(functools.partial(kernel, n, n_tp, conv), name='module_bac...]
    ppermute x9 -> x0, waiting for transfers between devices: 104 us -> none  [the longest x3 61.3 us: swap(): return lax.ppermute(value, 'pair', [(0, 1), (1, 0)])]
    reduce_scatter x3 -> x0, waiting for transfers between devices: 93.8 us -> none  [scatter_rows(): lax.psum_scatter(value.astype(BF16), 'outer', scatter_dimension=0, tiled=...]
    dot_general x8 -> x0, matrix products: 45.5 us -> none  [the longest x6 25.9 us: contract_tokens(): lax.dot_general(left, right, (((1,), (0,)), ((), ())), preferred_element_...]
    convert_element_type x4 -> x0, other arithmetic: 12.1 us -> none  [the longest x3 8.37 us: scatter_rows(): lax.psum_scatter(value.astype(BF16), 'outer', scatter_dimension=0, tiled=...]
    dynamic_slice x4 -> x0, local copies, waits for them, and re-layouts: 11.7 us -> none  [the longest x3 10.4 us: mine(): return lax.dynamic_index_in_dim(split, own, 1, keepdims=False)]
    ppermute x9 -> x0, starting transfers between devices: 6.72 us -> none  [the longest x3 3.93 us: scatter_channels(): lax.ppermute(part(me + step), 'tp', [(i, (i + step) % count) for i in ran...]
    unnamed x18 -> x0, local copies, waits for them, and re-layouts: 4.14 us -> none
  transfers between devices with their start and end apart: 12 -> 0, of which waited for: 9 -> 0; matrix products, arithmetic and copies ran while one was open for 16% -> 0% of each run, Pallas kernels for 0% -> 0%
where the time goes in v4:
time: 221 us
  Pallas kernels  220 us (100%)
    pallas_call x1, Pallas kernels, local(): pl.pallas_call(functools.partial(kernel, n, n_tp, conv), name='module_bac...  214 us
    pallas_call x1, Pallas kernels, local(): pl.pallas_call(write, name='write_results', grid=(parts,), out_shape=[jax...  5.69 us

profile of v4, /device:TPU:19, one launch (start us, length us, event | category | flops | bytes accessed | tf_op | source)
XLA Modules:
  0.0 220.8 jit_solution(11689152659408831189)
XLA Ops:
  0.6 214.3 %module_backward.1 = (bf16[512,1024]{1,0:T(8,128)(2,1)}, bf16[512,1024]{1,0:T(8,128)(2,1)}, bf16[512,1024]{1,0:T(8,128)(2,1)}, bf16[512,1024]{1,0:T(8,128)(2,1)}...) custom-call(bf16[512,1024]{1,0:T(8,128)(2,1)} %x_ref.1, ...), custom_call_target="tpu_custom_call" | custom-call | flops 34359738368 | bytes 83886080 | tf_op jit(solution)/shard_map/module_backward/pallas_call | solution.py:756
  215.0 5.7 %write_results.1 = (bf16[512,1024]{1,0:T(8,128)(2,1)}, f32[512,1024]{1,0:T(8,128)}, f32[512,1024]{1,0:T(8,128)}, f32[512,1024]{1,0:T(8,128)}, f32[31,1024]{1,0:T(8,128)}, /*index=5*/f32[1,1024]{1,0:T(1,128)}) custom-call(bf16[512,1024]{1,0:T(8,128)(2,1)} %get-tuple-element.18.refs_0_, bf16[512,1024]{1,0:T(8,128)(2,1)} %get-tuple-element.19.refs_1_, ...), custom_call_target="tpu_custom_call" | custom-call | bytes 11534336 | tf_op jit(solution)/shard_map/write_results/pallas_call | solution.py:795

commit v5 on v4

--- a/solution.py
+++ b/solution.py
@@ -638,7 +638,7 @@
     loop(JOBS, own_rows)
     small_swap.wait_recv()
     for g in range(n):
-        group[g] = small[:, g * rows : (g + 1) * rows, :] + small_x[:, g * rows : (g + 1) * rows, :]
+        group[g] = (small[:, g * rows : (g + 1) * rows, :] + small_x[:, g * rows : (g + 1) * rows, :]).astype(BF16)
     group_in[z] = group[z]
     for step in range(1, n):
         other = lax.rem(z + step, n)
@@ -650,10 +650,10 @@
         for step in range(1, n):
             other = lax.rem(z + step, n)
             arrived(group_in.at[other], s1_recv.at[other])
-        value = group_in[0]
+        value = group_in[0].astype(F32)
         for other in range(1, n):
-            value = value + group_in[other]
-        group_all[z] = value
+            value = value + group_in[other].astype(F32)
+        group_all[z] = value.astype(BF16)
         for step in range(1, n):
             remote(group_all.at[z], group_all.at[z], s2_send.at[step], s2_recv.at[z], level(lax.rem(z + step, n))).start()
 
@@ -686,9 +686,9 @@
         kept = min(rows, conv - g * rows)
         for c in range(n_lane):
             columns = slice(c * LANES, (c + 1) * LANES)
-            taps_total[g * rows : g * rows + kept, columns] = group_all[g, c, :kept]
+            taps_total[g * rows : g * rows + kept, columns] = group_all[g, c].astype(F32)[:kept]
             if kept < rows:
-                gain_total[:, columns] = group_all[g, c, kept:]
+                gain_total[:, columns] = group_all[g, c].astype(F32)[kept:]
     outs.append(load(taps_total, taps_out, out_sems.at[1]))
     outs.append(load(gain_total, gain_out, out_sems.at[8]))
 
@@ -768,7 +768,7 @@
             bf(JOBS, width, half), bf(JOBS, width, half),
             *[wide(tokens, LANES)] * 4, *[wide(n_tp, 8, tokens)] * 2,
             wide(n_lane, conv + 1, LANES), wide(n_lane, conv + 1, LANES),
-            *[wide(n, n_lane, rows, LANES)] * 3, wide(conv, channels), wide(1, channels),
+            *[bf(n, n_lane, rows, LANES)] * 3, wide(conv, channels), wide(1, channels),
             dma(n_sends), dma(n_seq), dma(n_seq), dma(n_tp), dma(2, n, 2, n_y), dma(2), dma(2), dma(n_tp), dma(n_tp),
             dma(2, per), dma(2, 2), dma(n), dma(2, 2), dma(9),
             dma(2, JOBS, n), dma(JOBS, n), dma(JOBS, n + 1), dma(JOBS, n + 1), dma(JOBS), dma(JOBS), dma(JOBS), dma(JOBS),
@@ -782,7 +782,7 @@
             flops=2 * 8 * tokens * width * n_seq * channels, bytes_accessed=80 * 2**20, transcendentals=0
         ),
     )(inputs, grad_out, w_value, w_gate, w_out, taps, ln_gain.reshape(1, channels))
-    parts = 4
+    parts = 2
     block = lambda shape: pl.BlockSpec((shape[0] // parts, shape[1]), lambda i: (i, 0))
     fixed = lambda shape: pl.BlockSpec(shape, lambda i: (0, 0))
     shapes = [shape for shape, dtype in out_shapes[:6]]

time: 221 us -> 218 us (0.986)
  Pallas kernels: 220 us -> 216 us
    pallas_call x1, Pallas kernels: 214 us -> 212 us  [local(): pl.pallas_call(functools.partial(kernel, n, n_tp, conv), name='module_bac...]
where the time goes in v5:
time: 218 us; the launch traced here: 217 us
  Pallas kernels  216 us (99%)
    pallas_call x1, Pallas kernels, local(): pl.pallas_call(functools.partial(kernel, n, n_tp, conv), name='module_bac...  212 us
    pallas_call x1, Pallas kernels, local(): pl.pallas_call(write, name='write_results', grid=(parts,), out_shape=[jax...  4.96 us

profile of v5, /device:TPU:19, one launch (start us, length us, event | category | flops | bytes accessed | tf_op | source)
XLA Modules:
  0.0 217.2 jit_solution(13360766465903797479)
XLA Ops:
  0.6 211.5 %module_backward.1 = (bf16[512,1024]{1,0:T(8,128)(2,1)}, bf16[512,1024]{1,0:T(8,128)(2,1)}, bf16[512,1024]{1,0:T(8,128)(2,1)}, bf16[512,1024]{1,0:T(8,128)(2,1)}...) custom-call(bf16[512,1024]{1,0:T(8,128)(2,1)} %x_ref.1, ...), custom_call_target="tpu_custom_call" | custom-call | flops 34359738368 | bytes 83886080 | tf_op jit(solution)/shard_map/module_backward/pallas_call | solution.py:756
  212.2 5.0 %write_results.1 = (bf16[512,1024]{1,0:T(8,128)(2,1)}, f32[512,1024]{1,0:T(8,128)}, f32[512,1024]{1,0:T(8,128)}, f32[512,1024]{1,0:T(8,128)}, f32[31,1024]{1,0:T(8,128)}, /*index=5*/f32[1,1024]{1,0:T(1,128)}) custom-call(bf16[512,1024]{1,0:T(8,128)(2,1)} %get-tuple-element.18.refs_0_, bf16[512,1024]{1,0:T(8,128)(2,1)} %get-tuple-element.19.refs_1_, ...), custom_call_target="tpu_custom_call" | custom-call | bytes 11534336 | tf_op jit(solution)/shard_map/write_results/pallas_call | solution.py:795
